TPU v7x, 256 devices: a whole 4x4x8 slice. The times are simulated.
256 devices in a mesh: ep: 64 (over z, x, core), tp: 4 (over y).
Axes of the slice: x: 4, y: 4, z: 8, core: 2. Of those that a mesh axis runs over, the one named last changes fastest.
Arguments:
- queries: bfloat16 [16384, 1024], P('ep', 'tp'), may hold values from -256 to 256
- key_rows: bfloat16 [16384, 1024], P('ep', 'tp'), may hold values from -8 to 8
- value_rows: bfloat16 [16384, 1024], P('ep', 'tp'), may hold values from -6 to 6
- head_lambda: float32 [8], P('tp'), may hold values from 0.3 to 0.8
- sub_gain: float32 [128], replicated, may hold values from 0.1 to 1.9
- out_weight: bfloat16 [1024, 2048], P('tp'), may hold values from -0.1875 to 0.1875
- expert_input: bfloat16 [12288, 2048], P('ep'), may hold values from -6 to 6
- norm_gain: float32 [2048], replicated, may hold values from 0.1 to 1.9
- route_ids: int32 [12288, 2], P('ep'), may hold values from 0 to 63, all different within a row; in each aligned block of 192 rows (0 to 191, 192 to 383, ...) at most 10 rows name the same one
- route_weight: float32 [12288, 2], P('ep'), may hold values from 0.25 to 1
- gate_weight: bfloat16 [64, 2048, 3584], P('ep', None, 'tp'), may hold values from -0.125 to 0.125
- up_weight: bfloat16 [64, 2048, 3584], P('ep', None, 'tp'), may hold values from -0.125 to 0.125
- down_weight: bfloat16 [64, 3584, 2048], P('ep', 'tp'), may hold values from -0.09375 to 0.09375
Outputs:
- mixer_out: bfloat16 [16384, 2048], P(('ep', 'tp'))
- expert_out: bfloat16 [12288, 2048], P('ep', 'tp')
Inputs may be any that keep to these rules, and one draw needn't show every extreme that they name: `route_ids`: each row names 2 different experts. In each aligned block of 192 rows no expert is named by more than 10 rows, a bound that some block reaches.
All inputs are finite; a program needn't handle non-finite values.
Results may differ from a plain program's by a relative error of at most 0.014.
Values may be sent and summed in bfloat16 or wider, within the bound.
A program may use at most 256 MiB of HBM per device.

v0:
```python
import jax
import jax.numpy as jnp
from jax import lax
from jax.sharding import PartitionSpec as P

EPS = 1e-06


def joined_along(parts, dim):
    lengths = list(parts.shape[1:])
    lengths[dim] *= parts.shape[0]
    return jnp.moveaxis(parts, 0, dim).reshape(lengths)


def copy_for_each(array, axis):
    devices = lax.axis_size(axis)
    return lax.all_to_all(
        jnp.broadcast_to(array[None], (devices, *array.shape)), axis, 0, 0, tiled=True
    )


def collect(array, axis, dim):
    return joined_along(copy_for_each(array, axis), dim)


def mixer_half(queries, key_rows, value_rows, head_lambda, sub_gain, out_weight):
    rows_here = queries.shape[0]
    heads_here = head_lambda.shape[0]
    head_width = queries.shape[1] // (2 * heads_here)
    value_width = value_rows.shape[1] // heads_here
    scaling = head_width ** (-0.5)
    query_blocks = queries.reshape(rows_here, heads_here, 2, head_width)
    query_pos = lax.axis_index("ep") * rows_here + jnp.arange(rows_here, dtype=jnp.int32)
    row_max = jnp.full((heads_here, 2, rows_here), -1e30, jnp.float32)
    key_piece = lax.all_gather(key_rows, "ep", axis=0, tiled=True)
    value_piece = lax.all_gather(value_rows, "ep", axis=0, tiled=True)
    length = key_piece.shape[0]
    key_blocks = key_piece.reshape(length, heads_here, 2, head_width)
    value_blocks = value_piece.reshape(length, heads_here, value_width)
    scores = (
        jnp.einsum("qhmd,khmd->hmqk", query_blocks, key_blocks, preferred_element_type=jnp.float32)
        * scaling
    )
    allowed = query_pos[:, None] >= jnp.arange(length, dtype=jnp.int32)[None, :]
    scores = jnp.where(allowed, scores, -1e30)
    new_max = jnp.maximum(row_max, jnp.max(scores, axis=-1))
    weights = jnp.where(allowed, jnp.exp(scores - new_max[..., None]), 0.0)
    row_total = jnp.sum(weights, axis=-1)
    numerator = jnp.einsum(
        "hmqk,khd->hmqd",
        weights.astype(jnp.bfloat16),
        value_blocks,
        preferred_element_type=jnp.float32,
    )
    row_max, row_total, numerator = (new_max, row_total, numerator)
    per_map = numerator / row_total[..., None]
    contrast = per_map[:, 0] - head_lambda[:, None, None] * per_map[:, 1]
    normed = (
        contrast * lax.rsqrt(jnp.mean(contrast * contrast, axis=-1, keepdims=True) + EPS) * sub_gain
    ).astype(jnp.bfloat16)
    attended = jnp.transpose(normed, (1, 0, 2)).reshape(rows_here, heads_here * value_width)
    return lax.psum_scatter(
        jnp.dot(attended, out_weight, preferred_element_type=jnp.float32).astype(jnp.bfloat16),
        "tp",
        scatter_dimension=0,
        tiled=True,
    )


def expert_half(
    expert_input, norm_gain, route_ids, route_weight, gate_weight, up_weight, down_weight
):
    rows_here, model_width = expert_input.shape
    experts = lax.axis_size("ep")
    top_count = route_ids.shape[1]
    capacity = 5 * top_count * rows_here // (3 * experts)
    slots = experts * capacity
    wide_rows = expert_input.astype(jnp.float32)
    normed = (
        wide_rows
        * lax.rsqrt(jnp.mean(wide_rows * wide_rows, axis=-1, keepdims=True) + EPS)
        * norm_gain
    ).astype(jnp.bfloat16)
    flat_ids = route_ids.reshape(-1)
    onehot = (flat_ids[:, None] == jnp.arange(experts, dtype=jnp.int32)[None, :]).astype(jnp.int32)
    rank_before = jnp.cumsum(onehot, axis=0) - onehot
    slot_index = jnp.sum(rank_before * onehot, axis=1)
    buffer_pos = (flat_ids * capacity + slot_index).reshape(rows_here, top_count)
    matches = buffer_pos[None, :, :] == jnp.arange(slots, dtype=jnp.int32)[:, None, None]
    dispatch = jnp.any(matches, axis=-1).astype(jnp.bfloat16)
    combine = jnp.sum(jnp.where(matches, route_weight[None, :, :], 0.0), axis=-1)
    gate_mat = gate_weight[0]
    up_mat = up_weight[0]
    down_mat = down_weight[0]
    column_share = model_width // lax.axis_size("tp")
    own_cols = lax.dynamic_slice_in_dim(
        normed, lax.axis_index("tp") * column_share, column_share, 1
    )
    outgoing = jnp.dot(dispatch, own_cols, preferred_element_type=jnp.float32).astype(jnp.bfloat16)
    arrived = lax.all_to_all(
        outgoing.reshape(experts, capacity, column_share),
        "ep",
        split_axis=0,
        concat_axis=0,
        tiled=True,
    ).reshape(slots, column_share)
    pieces = collect(arrived, "tp", 1)
    gate_act = jnp.dot(pieces, gate_mat, preferred_element_type=jnp.float32)
    up_act = jnp.dot(pieces, up_mat, preferred_element_type=jnp.float32)
    hidden = (jax.nn.silu(gate_act) * up_act).astype(jnp.bfloat16)
    partial_result = jnp.dot(hidden, down_mat, preferred_element_type=jnp.float32)
    summed = lax.psum_scatter(
        partial_result.astype(jnp.bfloat16), "tp", scatter_dimension=1, tiled=True
    )
    col_count = summed.shape[1]
    returned = lax.all_to_all(
        summed.reshape(experts, capacity, col_count), "ep", split_axis=0, concat_axis=0, tiled=True
    ).reshape(slots, col_count)
    mixed = lax.dot_general(
        combine,
        returned.astype(jnp.float32),
        (((0,), (0,)), ((), ())),
        preferred_element_type=jnp.float32,
    )
    return mixed.astype(jnp.bfloat16)


def shards(
    queries,
    key_rows,
    value_rows,
    head_lambda,
    sub_gain,
    out_weight,
    expert_input,
    norm_gain,
    route_ids,
    route_weight,
    gate_weight,
    up_weight,
    down_weight,
):
    mixer_out = mixer_half(queries, key_rows, value_rows, head_lambda, sub_gain, out_weight)
    expert_out = expert_half(
        expert_input, norm_gain, route_ids, route_weight, gate_weight, up_weight, down_weight
    )
    return (mixer_out, expert_out)


def solution(mesh):
    placed = (
        P("ep", "tp"),
        P("ep", "tp"),
        P("ep", "tp"),
        P("tp"),
        P(),
        P("tp", None),
        P("ep", None),
        P(),
        P("ep", None),
        P("ep", None),
        P("ep", None, "tp"),
        P("ep", None, "tp"),
        P("ep", "tp", None),
    )
    return jax.shard_map(
        shards,
        mesh=mesh,
        in_specs=placed,
        out_specs=(P(("ep", "tp"), None), P("ep", "tp")),
        check_vma=False,
    )
```

profile of v0, /device:TPU:2, one launch (start us, length us, event | category | flops | bytes accessed | tf_op | source)
XLA Modules:
  0.0 275.2 jit_solution(8443543517170979029)
XLA Ops:
  8.0 0.0 copy-start
  8.0 0.0 copy-start.1
  8.0 0.0 all-gather.3.cloned.1.call-start
  8.1 0.7 all-gather.3.cloned.1.call-update
  8.8 0.0 all-gather.5.cloned.1.call-start
  8.8 0.7 all-gather.5.cloned.1.call-update
  9.5 0.8 copy.47
  10.3 0.1 eq.38
  10.5 0.1 eq.42
  10.6 0.9 reduce-window.6
  11.5 0.2 slice_reduce_fusion
  11.8 0.1 fusion.32
  11.9 0.1 reduce_sum.50
  12.1 0.0 copy-start.2
  12.1 0.1 copy.50
  12.1 1.3 convert_element_type.41
  13.5 0.8 dynamic-slice
  14.2 0.7 multiply_add_fusion
  14.9 0.1 fusion.20
  15.1 0.0 copy-done.1
  15.1 0.2 multiply_reduce_fusion
  15.3 0.5 convolution_convert_fusion.1
  15.8 1.3 reshape.86
  17.1 12.0 %all-to-all-start = ((bf16[64,10,512]{2,1,0:T(8,128)(2,1)}), bf16[64,10,512]{2,1,0:T(8,128)(2,1)S(1)}, u32[]{:S(2)}, u32[]{:S(2)}) async-start(bf16[64,10,512]{2,1,0:T(8,128)(2,1)} %reshape.86), calls=%async_computation.1 | async-start | bytes 2097152 | tf_op jit(solution)/shard_map/all_to_all | solution.py:100
  29.1 0.0 copy-done.2
  29.1 0.1 copy.43
  29.2 32.8 %all-to-all-done = bf16[64,10,512]{2,1,0:T(8,128)(2,1)S(1)} async-done(((bf16[64,10,512]{2,1,0:T(8,128)(2,1)}), bf16[64,10,512]{2,1,0:T(8,128)(2,1)S(1)}, u32[]{:S(2)}, u32[]{:S(2)}) %all-to-all-start) | async-done | bytes 655392 | tf_op jit(solution)/shard_map/all_to_all | solution.py:100
  62.1 0.2 broadcast_in_dim.52
  62.3 0.3 copy.51
  62.6 1.9 broadcast_in_dim.53
  64.5 4.6 %all-to-all-start.1 = ((bf16[4,640,512]{1,2,0:T(8,128)(2,1)}), bf16[4,640,512]{1,2,0:T(8,128)(2,1)}, u32[]{:S(2)}, u32[]{:S(2)}) async-start(bf16[4,640,512]{1,2,0:T(8,128)(2,1)} %broadcast_in_dim.53), calls=%async_computation.2 | async-start | bytes 5242880 | tf_op jit(solution)/shard_map/all_to_all | solution.py:17
  69.1 0.2 reduce-scatter.5.cloned.1.call-start
  69.3 4.5 %iota_compare_fusion = pred[256,16384]{1,0:T(8,128)(4,1)} fusion(s32[256]{0:T(256)S(1)} %iota_add_fusion), kind=kLoop, calls=%fused_computation.7 | loop fusion | flops 4194304 | bytes 4195328 | tf_op jit(solution)/shard_map/ge | solution.py:44
  73.8 26.7 %all-to-all-done.1 = bf16[4,640,512]{1,2,0:T(8,128)(2,1)} async-done(((bf16[4,640,512]{1,2,0:T(8,128)(2,1)}), bf16[4,640,512]{1,2,0:T(8,128)(2,1)}, u32[]{:S(2)}, u32[]{:S(2)}) %all-to-all-start.1) | async-done | bytes 2621472 | tf_op jit(solution)/shard_map/all_to_all | solution.py:17
  100.4 7.2 %fusion.10 = f32[640,896]{1,0:T(8,128)} fusion(bf16[640,2048]{0,1:T(8,128)(2,1)} %bitcast.11, bf16[1,2048,896]{2,1,0:T(8,128)(2,1)} %param.23), kind=kOutput, calls=%fused_computation.12 | convolution fusion | flops 2348810240 | bytes 8585216 | tf_op jit(solution)/shard_map/dot_general | solution.py:108
  107.6 11.9 %fusion.12 = bf16[640,2048]{1,0:T(8,128)(2,1)} fusion(bf16[1,896,2048]{2,1,0:T(8,128)(2,1)} %param.25, f32[640,896]{1,0:T(8,128)} %fusion.10, bf16[640,2048]{0,1:T(8,128)(2,1)} %bitcast.11, bf16[1,2048,896]{2,1,0:T(8,128)(2,1)} %param.24), kind=kOutput, calls=%fused_computation.14 | convolution fusion | flops 4702371840 | bytes 14876672 | tf_op jit(solution)/shard_map/dot_general | solution.py:111
  119.5 0.0 reduce-scatter.5.cloned.1.call-update
  119.5 0.3 reduce-scatter.3.cloned.1.call-start
  119.8 0.0 all-gather.3.cloned.1.call-done
  119.8 11.8 %copy.44 = bf16[16384,256]{0,1:T(8,128)(2,1)} copy(bf16[16384,256]{1,0:T(8,128)(2,1)} %all-gather.3.cloned.1.call-done) | data formatting | bytes 16777216 | tf_op jit(solution)/shard_map/all_gather | solution.py:35
  131.6 31.3 %fusion = (f32[2,2,256]{2,1,0:T(2,128)S(1)}, f32[2,2,256,16384]{3,2,1,0:T(8,128)}) fusion(pred[256,16384]{1,0:T(8,128)(4,1)} %iota_compare_fusion, bf16[256,2,2,64]{0,3,2,1:T(8,128)(2,1)S(1)} %bitcast.81, bf16[16384,2,2,64]{0,3,2,1:T(8,128)(2,1)} %bitcast.79), kind=kOutput, calls=%fused_computation.2 | convolution fusion | flops 2197814272 | bytes 79826944 | tf_op jit(solution)/shard_map/qhmd,khmd->hmqk/dot_general | solution.py:41
  162.9 24.2 %fusion.1 = f32[2,2,256]{2,1,0:T(2,128)S(1)} fusion(f32[2,2,256,16384]{3,2,1,0:T(8,128)} %get-tuple-element.3, f32[2,2,256]{2,1,0:T(2,128)S(1)} %broadcast_maximum_fusion, pred[256,16384]{1,0:T(8,128)(4,1)} %iota_compare_fusion), kind=kLoop, calls=%fused_computation.3 | loop fusion | flops 83885056 | bytes 71311360 | tf_op jit(solution)/shard_map/reduce_sum | solution.py:48
  187.1 0.0 all-gather.5.cloned.1.call-done
  187.2 12.0 %copy.45 = bf16[16384,256]{0,1:T(8,128)(2,1)} copy(bf16[16384,256]{1,0:T(8,128)(2,1)} %all-gather.5.cloned.1.call-done) | data formatting | bytes 16777216 | tf_op jit(solution)/shard_map/all_gather | solution.py:36
  199.1 0.0 copy-start.4
  199.1 0.0 copy-start.5
  199.1 28.4 %fusion.17 = f32[2,2,256,128]{2,3,1,0:T(8,128)S(1)} fusion(bf16[16384,2,128,1]{0,2,3,1:T(8,128)(2,1)} %bitcast.78, f32[2,2,256,16384]{3,2,1,0:T(8,128)} %get-tuple-element.3, f32[2,2,256]{2,1,0:T(2,128)S(1)} %broadcast_maximum_fusion, pred[256,16384]{1,0:T(8,128)(4,1)} %iota_compare_fusion, f32[2,2,256]{2,1,0:T(2,128)S(1)} %fusion.1), kind=kOutput, calls=%fused_computation.19 | convolution fusion | flops 4378984448 | bytes 80224256 | tf_op jit(solution)/shard_map/hmqk,khd->hmqd/dot_general | solution.py:49
  227.5 0.0 copy-done.4
  227.6 0.0 copy-start.3
  227.6 0.1 multiply_reduce_fusion.1
  227.7 0.0 copy-done.5
  227.7 0.1 multiply_convert_fusion.1
  227.8 0.0 copy-done
  227.8 1.5 convolution_convert_fusion
  229.3 0.0 reduce-scatter.3.cloned.1.call-update
  229.3 0.0 reduce-scatter.5.cloned.1.call-done
  229.3 2.2 reshape.88
  231.5 6.3 %all-to-all-start.2 = ((bf16[64,10,512]{2,1,0:T(8,128)(2,1)}), bf16[64,10,512]{2,1,0:T(8,128)(2,1)S(1)}, u32[]{:S(2)}, u32[]{:S(2)}) async-start(bf16[64,10,512]{2,1,0:T(8,128)(2,1)} %reshape.88), calls=%async_computation.4 | async-start | bytes 2097152 | tf_op jit(solution)/shard_map/all_to_all | solution.py:116
  237.8 0.0 copy-done.3
  237.8 0.2 select_reduce_fusion
  238.0 28.6 %all-to-all-done.2 = bf16[64,10,512]{2,1,0:T(8,128)(2,1)S(1)} async-done(((bf16[64,10,512]{2,1,0:T(8,128)(2,1)}), bf16[64,10,512]{2,1,0:T(8,128)(2,1)S(1)}, u32[]{:S(2)}, u32[]{:S(2)}) %all-to-all-start.2) | async-done | bytes 655392 | tf_op jit(solution)/shard_map/all_to_all | solution.py:116
  266.6 0.2 reshape.89
  266.8 1.0 fusion.39
  267.8 0.0 reduce-scatter.3.cloned.1.call-done
  (6 shorter events, 0.1 us)
Async XLA Ops:
  8.0 219.8 %copy-start = (bf16[256,2048]{1,0:T(8,128)(2,1)S(1)}, bf16[256,2048]{1,0:T(8,128)(2,1)}, u32[]{:S(2)}) copy-start(bf16[256,2048]{1,0:T(8,128)(2,1)} %param.18) | copy-start | bytes 3145732
  8.0 7.1 %copy-start.1 = (bf16[192,2048]{1,0:T(8,128)(2,1)S(1)}, bf16[192,2048]{1,0:T(8,128)(2,1)}, u32[]{:S(2)}) copy-start(bf16[192,2048]{1,0:T(8,128)(2,1)} %param.19) | copy-start | bytes 2359300
  8.0 111.8 %all-gather.3.cloned.1.call-start = ((), (), s32[]{:S(2)}) async-start(), calls=%async_computation.5 | async-start | bytes 8519680 | tf_op jit(solution)/shard_map/all_gather | solution.py:35
  8.8 178.4 %all-gather.5.cloned.1.call-start = ((), (), s32[]{:S(2)}) async-start(), calls=%async_computation.6 | async-start | bytes 8519680 | tf_op jit(solution)/shard_map/all_gather | solution.py:36
  12.1 17.0 %copy-start.2 = (bf16[256,256]{1,0:T(8,128)(2,1)S(1)}, bf16[256,256]{1,0:T(8,128)(2,1)}, u32[]{:S(2)}) copy-start(bf16[256,256]{1,0:T(8,128)(2,1)} %param.13) | copy-start | bytes 393220
  17.1 45.0 %all-to-all-start = ((bf16[64,10,512]{2,1,0:T(8,128)(2,1)}), bf16[64,10,512]{2,1,0:T(8,128)(2,1)S(1)}, u32[]{:S(2)}, u32[]{:S(2)}) async-start(bf16[64,10,512]{2,1,0:T(8,128)(2,1)} %reshape.86), calls=%async_computation.1 | async-start | bytes 2097152 | tf_op jit(solution)/shard_map/all_to_all | solution.py:100
  64.5 35.9 %all-to-all-start.1 = ((bf16[4,640,512]{1,2,0:T(8,128)(2,1)}), bf16[4,640,512]{1,2,0:T(8,128)(2,1)}, u32[]{:S(2)}, u32[]{:S(2)}) async-start(bf16[4,640,512]{1,2,0:T(8,128)(2,1)} %broadcast_in_dim.53), calls=%async_computation.2 | async-start | bytes 5242880 | tf_op jit(solution)/shard_map/all_to_all | solution.py:17
  69.1 160.3 %reduce-scatter.5.cloned.1.call-start = ((), (), s32[]{:S(2)}) async-start(), calls=%async_computation.8 | async-start | bytes 3276800 | tf_op jit(solution)/shard_map/reduce_scatter | solution.py:112
  119.5 148.3 %reduce-scatter.3.cloned.1.call-start = ((), (), s32[]{:S(2)}) async-start(), calls=%async_computation.7 | async-start | bytes 1310720 | tf_op jit(solution)/shard_map/reduce_scatter | solution.py:62
  199.1 28.4 %copy-start.4 = (f32[2]{0:T(128)S(1)}, f32[2]{0:T(128)}, u32[]{:S(2)}) copy-start(f32[2]{0:T(128)} %param.16) | copy-start | bytes 28
  199.1 28.6 %copy-start.5 = (f32[128]{0:T(128)S(1)}, f32[128]{0:T(128)}, u32[]{:S(2)}) copy-start(f32[128]{0:T(128)} %param.17) | copy-start | bytes 1540
  227.6 10.2 %copy-start.3 = (f32[192,2]{0,1:T(2,128)S(1)}, f32[192,2]{0,1:T(2,128)}, u32[]{:S(2)}) copy-start(f32[192,2]{0,1:T(2,128)} %param.22) | copy-start | bytes 4612
  231.5 35.0 %all-to-all-start.2 = ((bf16[64,10,512]{2,1,0:T(8,128)(2,1)}), bf16[64,10,512]{2,1,0:T(8,128)(2,1)S(1)}, u32[]{:S(2)}, u32[]{:S(2)}) async-start(bf16[64,10,512]{2,1,0:T(8,128)(2,1)} %reshape.88), calls=%async_computation.4 | async-start | bytes 2097152 | tf_op jit(solution)/shard_map/all_to_all | solution.py:116
Sparse Core Ops, SparseCore 0:
  11.6 88.4 all-gather.2
  102.9 79.7 all-gather.4
Sparse Core Ops, SparseCore 1:
  119.6 31.8 reduce-scatter.4
  229.4 21.7 reduce-scatter.2
where the time goes:
time: 277 us; the launch traced here: 275 us
  waiting for transfers between devices  89.5 us (32%)
  matrix products  81.7 us (29%)
  other arithmetic  32.6 us (12%)
  local copies, waits for them, and re-layouts  32.2 us (12%)
  starting transfers between devices  23.4 us (8%)
  between operations  15.8 us (6%)
    all_to_all x1, waiting for transfers between devices, expert_half(): lax.all_to_all(outgoing.reshape(experts, capacity, column_share), 'ep', s...  32.8 us
    dot_general x1, matrix products, mixer_half(): jnp.einsum('qhmd,khmd->hmqk', query_blocks, key_blocks, preferred_element...  31.3 us
    all_to_all x1, waiting for transfers between devices, expert_half(): lax.all_to_all(summed.reshape(experts, capacity, col_count), 'ep', split_...  28.6 us
    dot_general x1, matrix products, mixer_half(): jnp.einsum('hmqk,khd->hmqd', weights.astype(jnp.bfloat16), value_blocks,...  28.4 us
    all_to_all x1, waiting for transfers between devices, copy_for_each(): lax.all_to_all(jnp.broadcast_to(array[None], (devices, *array.shape)), ax...  26.7 us
    reduce_sum x1, other arithmetic, mixer_half(): row_total = jnp.sum(weights, axis=-1)  24.2 us
    all_to_all x1, starting transfers between devices, expert_half(): lax.all_to_all(outgoing.reshape(experts, capacity, column_share), 'ep', s...  12 us
    all_gather x1, local copies, waits for them, and re-layouts, mixer_half(): value_piece = lax.all_gather(value_rows, 'ep', axis=0, tiled=True)  12 us
  transfers between devices with their start and end apart: 7, of which 3 were waited for; matrix products, arithmetic and copies ran while one was open for 53% of the time, Pallas kernels for 0%

commit v1 on v0

v1 whole, which is shorter than its diff:
```python
import functools
import math

import jax
import jax.numpy as jnp
from jax import lax
from jax.experimental import pallas as pl
from jax.experimental.pallas import tpu as pltpu
from jax.sharding import Mesh, PartitionSpec as P

EPS = 1e-06
NZ, NX, NC, NT = 8, 4, 2, 4
EP = ("z", "x", "core")
BLOCK = 256
HALF = BLOCK // 2
CHUNK = NC * BLOCK
COLS = 2 * NX * HALF
ACC = 144
LOW = -1e30
EXP2_SCALE = 64 ** (-0.5) * math.log2(math.e)


def pieces_of(value):
    first = value.astype(jnp.bfloat16).astype(jnp.float32)
    second = (value - first).astype(jnp.bfloat16).astype(jnp.float32)
    third = value - first - second
    return first, second, third


def flash_kernel(query_ref, pair_ref, out_ref, rhs_ref, max_ref, acc_ref):
    z, x, core = lax.axis_index("z"), lax.axis_index("x"), lax.axis_index("core")
    map_row = lax.broadcasted_iota(jnp.int32, (128, HALF), 0)
    ones = jnp.ones((ACC - 128, CHUNK), jnp.bfloat16)
    tile = 256

    for group in range(2):
        query_z = z if group == 0 else NZ - 1 - z
        for head in range(2):
            for step in range(NX):
                block = query_ref[group, step, head * 128 : (head + 1) * 128, :]
                for which in range(2):
                    first = (which * NX + step) * HALF
                    keep = (map_row < 64) if which == 0 else (map_row >= 64)
                    rhs_ref[:, first : first + HALF] = jnp.where(
                        keep, block, jnp.zeros_like(block)
                    )
            max_ref[...] = jnp.full_like(max_ref, LOW)
            acc_ref[...] = jnp.zeros_like(acc_ref)

            def work(step_z, masked):
                keys, values = [], []
                for c in range(NC):
                    keys.append(
                        pair_ref[step_z * NC + c, 0:256, head * 128 : (head + 1) * 128]
                    )
                    values.append(
                        pair_ref[step_z * NC + c, 256 + head * 128 : 256 + (head + 1) * 128, :]
                    )
                keys = jnp.concatenate(keys, axis=0)
                values = jnp.concatenate([jnp.concatenate(values, axis=1), ones], axis=0)
                for first in range(0, COLS, tile):
                    cols = slice(first, first + tile)
                    scores = jnp.dot(keys, rhs_ref[:, cols], preferred_element_type=jnp.float32)
                    if masked:
                        key = lax.broadcasted_iota(jnp.int32, (CHUNK, tile), 0)
                        key = key + 2 * BLOCK * x
                        col = lax.broadcasted_iota(jnp.int32, (CHUNK, tile), 1) + first
                        shift = (col // HALF) % NX
                        query_x = lax.rem(x - shift + NX, NX)
                        position = (2 * query_x + core) * BLOCK + group * HALF + col % HALF
                        scores = jnp.where(position >= key, scores, -3e38)
                    before = max_ref[0:1, cols]
                    now = jnp.maximum(before, jnp.max(scores, axis=0, keepdims=True))
                    weights = jnp.exp2((scores - now) * EXP2_SCALE).astype(jnp.bfloat16)
                    rescale = jnp.exp2((before - now) * EXP2_SCALE)
                    max_ref[0:1, cols] = now
                    acc_ref[:, cols] = acc_ref[:, cols] * rescale + jnp.dot(
                        values, weights, preferred_element_type=jnp.float32
                    )

            lax.fori_loop(0, query_z, lambda s, c: (work(s, False), c)[1], 0)
            work(query_z, True)

            row = lax.broadcasted_iota(jnp.int32, (ACC - 128, COLS), 0)
            stats = jnp.zeros((ACC - 128, COLS), jnp.float32)
            rows = pieces_of(acc_ref[128:129, :]) + pieces_of(max_ref[0:1, :])
            for index, piece in enumerate(rows):
                stats = jnp.where(row == index, piece, stats)
            for which in range(2):
                for step in range(NX):
                    first = (which * NX + step) * HALF
                    lanes = slice(group * HALF, (group + 1) * HALF)
                    out_ref[step, 2 * head + which, 0:128, lanes] = acc_ref[
                        0:128, first : first + HALF
                    ].astype(jnp.bfloat16)
                    out_ref[step, 2 * head + which, 128:ACC, lanes] = stats[
                        :, first : first + HALF
                    ].astype(jnp.bfloat16)


def flash(query_parts, pairs):
    return pl.pallas_call(
        flash_kernel,
        out_shape=jax.ShapeDtypeStruct((NX, 4, ACC, BLOCK), jnp.bfloat16),
        in_specs=[pl.BlockSpec(memory_space=pltpu.VMEM)] * 2,
        out_specs=pl.BlockSpec(memory_space=pltpu.VMEM),
        scratch_shapes=[
            pltpu.VMEM((128, COLS), jnp.bfloat16),
            pltpu.VMEM((8, COLS), jnp.float32),
            pltpu.VMEM((ACC, COLS), jnp.float32),
        ],
        compiler_params=pltpu.CompilerParams(vmem_limit_bytes=40 * 2**20),
        cost_estimate=pl.CostEstimate(
            flops=15_000_000_000, bytes_accessed=6_000_000, transcendentals=9_400_000
        ),
        name="flash",
    )(query_parts, pairs)


def merge_kernel(lambda_ref, gain_ref, own_ref, one_ref, two_ref, three_ref, out_ref):
    parts = (own_ref, one_ref, two_ref, three_ref)
    for head in range(2):
        per_map = []
        for which in range(2):
            index = 2 * head + which
            totals, maxima = [], []
            for part in parts:
                stats = part[index, 128:ACC, :].astype(jnp.float32)
                totals.append(stats[0:1] + stats[1:2] + stats[2:3])
                maxima.append(stats[3:4] + stats[4:5] + stats[5:6])
            largest = functools.reduce(jnp.maximum, maxima)
            total, numerator = 0.0, 0.0
            for part, own_total, own_max in zip(parts, totals, maxima):
                factor = jnp.exp2((own_max - largest) * EXP2_SCALE)
                total = total + factor * own_total
                numerator = numerator + factor * part[index, 0:128, :].astype(jnp.float32)
            per_map.append(numerator / total)
        contrast = per_map[0] - lambda_ref[head] * per_map[1]
        square = jnp.mean(contrast * contrast, axis=0, keepdims=True)
        normed = contrast * lax.rsqrt(square + EPS) * gain_ref[...]
        out_ref[head * 128 : (head + 1) * 128, :] = normed.astype(jnp.bfloat16)


def merge(head_lambda, sub_gain, parts):
    return pl.pallas_call(
        merge_kernel,
        out_shape=jax.ShapeDtypeStruct((BLOCK, BLOCK), jnp.bfloat16),
        in_specs=[pl.BlockSpec(memory_space=pltpu.SMEM)]
        + [pl.BlockSpec(memory_space=pltpu.VMEM)] * 5,
        out_specs=pl.BlockSpec(memory_space=pltpu.VMEM),
        name="merge",
    )(head_lambda, sub_gain[:, None], *parts)


def moved(array, shift, flip):
    pairs = []
    for z in range(NZ):
        for x in range(NX):
            to_z = NZ - 1 - z if flip else z
            pairs.append((z * NX + x, to_z * NX + (x + shift) % NX))
    return lax.ppermute(array, ("z", "x"), pairs)


def mixer_half(queries, key_rows, value_rows, head_lambda, sub_gain, out_weight):
    pair = jnp.concatenate([key_rows, value_rows.T], axis=0)
    pairs = lax.all_gather(pair, ("z", "core"), axis=0, tiled=False)
    flipped = queries.T
    lower, upper = flipped[:, :HALF], flipped[:, HALF:]
    parts = [lower] + [moved(lower, s, False) for s in range(1, NX)]
    parts += [moved(upper, s, True) for s in range(NX)]
    query_parts = jnp.stack(parts).reshape(2, NX, BLOCK, HALF)
    partial = flash(query_parts, pairs)
    parts = [partial[0]] + [moved(partial[s], -s, False) for s in range(1, NX)]
    attended = merge(head_lambda, sub_gain, parts)
    attended = jnp.concatenate(
        [attended[:, :HALF], moved(attended[:, HALF:], 0, True)], axis=1
    )
    part = lax.dot_general(
        attended, out_weight, (((0,), (0,)), ((), ())), preferred_element_type=jnp.float32
    ).astype(jnp.bfloat16)
    return lax.psum_scatter(part, "tp", scatter_dimension=0, tiled=True)


def expert_half(
    expert_input, norm_gain, route_ids, route_weight, gate_weight, up_weight, down_weight
):
    rows_here, model_width = expert_input.shape
    experts = lax.axis_size(EP)
    top_count = route_ids.shape[1]
    capacity = 5 * top_count * rows_here // (3 * experts)
    slots = experts * capacity
    wide_rows = expert_input.astype(jnp.float32)
    normed = (
        wide_rows
        * lax.rsqrt(jnp.mean(wide_rows * wide_rows, axis=-1, keepdims=True) + EPS)
        * norm_gain
    ).astype(jnp.bfloat16)
    flat_ids = route_ids.reshape(-1)
    onehot = (flat_ids[:, None] == jnp.arange(experts, dtype=jnp.int32)[None, :]).astype(jnp.int32)
    rank_before = jnp.cumsum(onehot, axis=0) - onehot
    slot_index = jnp.sum(rank_before * onehot, axis=1)
    buffer_pos = (flat_ids * capacity + slot_index).reshape(rows_here, top_count)
    matches = buffer_pos[None, :, :] == jnp.arange(slots, dtype=jnp.int32)[:, None, None]
    dispatch = jnp.any(matches, axis=-1).astype(jnp.bfloat16)
    combine = jnp.sum(jnp.where(matches, route_weight[None, :, :], 0.0), axis=-1)
    gate_mat = gate_weight[0]
    up_mat = up_weight[0]
    down_mat = down_weight[0]
    column_share = model_width // lax.axis_size("tp")
    own_cols = lax.dynamic_slice_in_dim(
        normed, lax.axis_index("tp") * column_share, column_share, 1
    )
    outgoing = jnp.dot(dispatch, own_cols, preferred_element_type=jnp.float32).astype(jnp.bfloat16)
    arrived = lax.all_to_all(
        outgoing.reshape(experts, capacity, column_share),
        EP,
        split_axis=0,
        concat_axis=0,
        tiled=True,
    ).reshape(slots, column_share)
    pieces = lax.all_gather(arrived, "tp", axis=0, tiled=False)
    pieces = jnp.moveaxis(pieces, 0, 1).reshape(slots, model_width)
    gate_act = jnp.dot(pieces, gate_mat, preferred_element_type=jnp.float32)
    up_act = jnp.dot(pieces, up_mat, preferred_element_type=jnp.float32)
    hidden = (jax.nn.silu(gate_act) * up_act).astype(jnp.bfloat16)
    partial_result = jnp.dot(hidden, down_mat, preferred_element_type=jnp.float32)
    summed = lax.psum_scatter(
        partial_result.astype(jnp.bfloat16), "tp", scatter_dimension=1, tiled=True
    )
    col_count = summed.shape[1]
    returned = lax.all_to_all(
        summed.reshape(experts, capacity, col_count), EP, split_axis=0, concat_axis=0, tiled=True
    ).reshape(slots, col_count)
    mixed = lax.dot_general(
        combine,
        returned.astype(jnp.float32),
        (((0,), (0,)), ((), ())),
        preferred_element_type=jnp.float32,
    )
    return mixed.astype(jnp.bfloat16)


def shards(
    queries,
    key_rows,
    value_rows,
    head_lambda,
    sub_gain,
    out_weight,
    expert_input,
    norm_gain,
    route_ids,
    route_weight,
    gate_weight,
    up_weight,
    down_weight,
):
    mixer_out = mixer_half(queries, key_rows, value_rows, head_lambda, sub_gain, out_weight)
    expert_out = expert_half(
        expert_input, norm_gain, route_ids, route_weight, gate_weight, up_weight, down_weight
    )
    return (mixer_out, expert_out)


def solution(mesh):
    mesh = Mesh(mesh.devices.reshape(NZ, NX, NC, NT), (*EP, "tp"))
    placed = (
        P(EP, "tp"),
        P(EP, "tp"),
        P(EP, "tp"),
        P("tp"),
        P(),
        P("tp", None),
        P(EP, None),
        P(),
        P(EP, None),
        P(EP, None),
        P(EP, None, "tp"),
        P(EP, None, "tp"),
        P(EP, "tp", None),
    )
    return jax.shard_map(
        shards,
        mesh=mesh,
        in_specs=placed,
        out_specs=(P((*EP, "tp"), None), P(EP, "tp")),
        check_vma=False,
    )
```

time: 277 us -> 265 us (0.957)
  matrix products: 81.7 us -> 20.9 us
  blocking collectives: 0 us -> 40.7 us
  Pallas kernels: 0 us -> 34.2 us
  other arithmetic: 32.6 us -> 6.01 us
  local copies, waits for them, and re-layouts: 32.2 us -> 23.4 us
  starting transfers between devices: 23.4 us -> 30.2 us
  waiting for transfers between devices: 89.5 us -> 94.9 us
    dot_general x3 -> x1, matrix products: 61.2 us -> 1.45 us  [mixer_half(): lax.dot_general(attended, out_weight, (((0,), (0,)), ((), ())), preferred...]
    all_to_all x3 -> x1, waiting for transfers between devices: 88.1 us -> 28.6 us  [expert_half(): lax.all_to_all(summed.reshape(experts, capacity, col_count), EP, split_ax...]
    all_to_all x0 -> x1, blocking collectives: none -> 40.7 us  [expert_half(): lax.all_to_all(outgoing.reshape(experts, capacity, column_share), EP, spl...]
    all_gather x2, waiting for transfers between devices: 0.04 us -> 37.7 us  [the longest x1 33.5 us: expert_half(): pieces = lax.all_gather(arrived, 'tp', axis=0, tiled=False)]
    pallas_call x0 -> x2, Pallas kernels: none -> 34.2 us  [the longest x1 31.9 us: flash(): pl.pallas_call(flash_kernel, out_shape=jax.ShapeDtypeStruct((NX, 4, ACC,...]
    ppermute x0 -> x11, waiting for transfers between devices: none -> 28.6 us  [moved(): return lax.ppermute(array, ('z', 'x'), pairs)]
    reduce_sum x2 -> x0, other arithmetic: 24.3 us -> none  [the longest x1 24.2 us: mixer_half(): row_total = jnp.sum(weights, axis=-1)]
    ppermute x0 -> x11, starting transfers between devices: none -> 21.1 us  [moved(): return lax.ppermute(array, ('z', 'x'), pairs)]
  transfers between devices with their start and end apart: 7 -> 16, of which waited for: 3 -> 8; matrix products, arithmetic and copies ran while one was open for 53% -> 14% of each run, Pallas kernels for 0% -> 13%
where the time goes in v1:
time: 265 us; the launch traced here: 264 us
  waiting for transfers between devices  94.9 us (36%)
  blocking collectives  40.7 us (15%)
  Pallas kernels  34.2 us (13%)
  starting transfers between devices  30.2 us (11%)
  local copies, waits for them, and re-layouts  23.4 us (9%)
  matrix products  20.9 us (8%)
  between operations  14 us (5%)
  other arithmetic  6.01 us (2%)
    all_to_all x1, blocking collectives, expert_half(): lax.all_to_all(outgoing.reshape(experts, capacity, column_share), EP, spl...  40.7 us
    all_gather x1, waiting for transfers between devices, expert_half(): pieces = lax.all_gather(arrived, 'tp', axis=0, tiled=False)  33.5 us
    pallas_call x1, Pallas kernels, flash(): pl.pallas_call(flash_kernel, out_shape=jax.ShapeDtypeStruct((NX, 4, ACC,...  31.9 us
    ppermute x11, waiting for transfers between devices, moved(): return lax.ppermute(array, ('z', 'x'), pairs)  28.6 us
    all_to_all x1, waiting for transfers between devices, expert_half(): lax.all_to_all(summed.reshape(experts, capacity, col_count), EP, split_ax...  28.6 us
    ppermute x11, starting transfers between devices, moved(): return lax.ppermute(array, ('z', 'x'), pairs)  21.1 us
    dot_general x1, matrix products, expert_half(): jnp.dot(hidden, down_mat, preferred_element_type=jnp.float32)  11.3 us
    all_to_all x1, starting transfers between devices, expert_half(): lax.all_to_all(summed.reshape(experts, capacity, col_count), EP, split_ax...  8.86 us
  transfers between devices with their start and end apart: 16, of which 8 were waited for; matrix products, arithmetic and copies ran while one was open for 14% of the time, Pallas kernels for 13%

profile of v1, /device:TPU:2, one launch (start us, length us, event | category | flops | bytes accessed | tf_op | source)
XLA Modules:
  0.0 264.3 jit_solution(14217389998851166588)
XLA Ops:
  7.2 0.0 copy-start
  7.2 0.0 all-gather.4.cloned.1.call-start
  7.2 0.9 copy.58
  8.1 0.1 eq.42
  8.3 0.1 eq.38
  8.4 1.4 multiply_reduce_fusion
  9.8 2.5 convert_element_type.33
  12.3 0.9 reduce-window.6
  13.2 0.2 slice_reduce_fusion
  13.5 0.1 fusion.24
  13.6 0.1 reduce_sum.30
  13.7 0.1 copy.61
  13.8 0.2 fusion.11
  14.0 0.8 dynamic-slice
  14.7 1.4 convolution_convert_fusion.1
  16.2 0.2 reshape.55
  16.4 40.7 %all_to_all.10 = bf16[64,10,512]{2,1,0:T(8,128)(2,1)S(1)} all-to-all(bf16[64,10,512]{2,1,0:T(8,128)(2,1)S(1)} %reshape.55), channel_id=1, replica_groups=mesh['z'=8,'x'=4,'core'=2,'tp'=4] {'z','x','core'}, dimensions={0} | all-to-all | bytes 1310720 | tf_op jit(solution)/shard_map/all_to_all | solution.py:214
  57.1 1.1 all_gather_reshape.3
  58.2 0.0 all-gather.4.cloned.1.call-update
  58.2 0.0 all-gather.6.cloned.1.call-start
  58.3 0.1 copy.55
  58.4 0.7 pad_maximum_fusion
  59.1 0.0 all-gather.6.cloned.1.call-update
  59.2 0.0 reduce-scatter.5.cloned.1.call-start
  59.2 33.5 %all-gather.4.cloned.1.call-done = bf16[4,640,512]{2,1,0:T(8,128)(2,1)} async-done(((bf16[1,640,512]{2,1,0:T(8,128)(2,1)}), bf16[4,640,512]{2,1,0:T(8,128)(2,1)}) %all-gather.4.cloned.1.call-update) | async-done | bytes 2621456 | tf_op jit(solution)/shard_map/all_gather | solution.py:221
  92.7 4.4 %copy.62 = bf16[4,640,512]{1,2,0:T(8,128)(2,1)} copy(bf16[4,640,512]{2,1,0:T(8,128)(2,1)} %all-gather.4.cloned.1.call-done) | data formatting | bytes 5242880 | tf_op jit(solution)/shard_map/all_gather | solution.py:221
  97.1 5.7 %fusion.4 = f32[640,896]{1,0:T(8,128)S(1)} fusion(bf16[640,2048]{0,1:T(8,128)(2,1)} %bitcast.75, bf16[1,2048,896]{2,1,0:T(8,128)(2,1)} %param.23), kind=kOutput, calls=%fused_computation.4 | convolution fusion | flops 2348810240 | bytes 8585216 | tf_op jit(solution)/shard_map/dot_general | solution.py:223
  102.8 11.3 %fusion.6 = bf16[640,2048]{1,0:T(8,128)(2,1)} fusion(bf16[1,896,2048]{2,1,0:T(8,128)(2,1)} %param.25, f32[640,896]{1,0:T(8,128)S(1)} %fusion.4, bf16[640,2048]{0,1:T(8,128)(2,1)} %bitcast.76, bf16[1,2048,896]{2,1,0:T(8,128)(2,1)} %param.24), kind=kOutput, calls=%fused_computation.6 | convolution fusion | flops 4702371840 | bytes 14876672 | tf_op jit(solution)/shard_map/dot_general | solution.py:226
  114.1 0.0 reduce-scatter.5.cloned.1.call-update
  114.1 0.0 reduce-scatter.3.cloned.1.call-start
  114.2 0.8 copy-done.5
  115.0 2.2 collective-permute-start.1
  117.2 2.0 collective-permute-start.2
  119.2 5.4 %collective-permute-start.6 = (bf16[256,128]{0,1:T(8,128)(2,1)S(1)}, bf16[256,128]{0,1:T(8,128)(2,1)S(1)}, u32[]{:S(2)}, u32[]{:S(2)}) collective-permute-start(bf16[256,128]{0,1:T(8,128)(2,1)S(1)} %get-tuple-element.8), channel_id=1, source_target_pairs={{0,248},{8,224},{16,232},{24,240},{32,216},{40,192},{48,200},{56,2... | collective-permute-start | bytes 196616 | tf_op jit(solution)/shard_map/ppermute | solution.py:161
  124.6 3.6 %collective-permute-start.4 = (bf16[256,128]{0,1:T(8,128)(2,1)S(1)}, bf16[256,128]{0,1:T(8,128)(2,1)S(1)}, u32[]{:S(2)}, u32[]{:S(2)}) collective-permute-start(bf16[256,128]{0,1:T(8,128)(2,1)S(1)} %get-tuple-element.8), channel_id=1, source_target_pairs={{0,232},{8,240},{16,248},{24,224},{32,200},{40,208},{48,216},{56,1... | collective-permute-start | bytes 196616 | tf_op jit(solution)/shard_map/ppermute | solution.py:161
  128.3 0.7 collective-permute-start.3
  129.0 13.0 %collective-permute-done.3 = bf16[256,128]{0,1:T(8,128)(2,1)S(1)} collective-permute-done((bf16[256,128]{0,1:T(8,128)(2,1)S(1)}, bf16[256,128]{0,1:T(8,128)(2,1)S(1)}, u32[]{:S(2)}, u32[]{:S(2)}) %collective-permute-start.3) | collective-permute-done | bytes 65568 | tf_op jit(solution)/shard_map/ppermute | solution.py:161
  142.0 0.3 copy.54
  142.3 4.2 %all-gather.6.cloned.1.call-done = bf16[8192,256]{0,1:T(8,128)(2,1)} async-done(((bf16[512,256]{0,1:T(8,128)(2,1)}), bf16[8192,256]{0,1:T(8,128)(2,1)}) %all-gather.6.cloned.1.call-update) | async-done | bytes 4194320 | tf_op jit(solution)/shard_map/all_gather | solution.py:166
  146.5 6.4 %copy.56 = bf16[8192,256]{1,0:T(8,128)(2,1)} copy(bf16[8192,256]{0,1:T(8,128)(2,1)} %all-gather.6.cloned.1.call-done) | data formatting | bytes 8388608 | tf_op jit(solution)/shard_map/all_gather | solution.py:166
  152.9 2.2 copy-done.1
  155.1 31.9 %flash.1 = bf16[4,4,144,256]{3,2,1,0:T(8,128)(2,1)S(1)} custom-call(bf16[2,4,256,128]{3,2,1,0:T(8,128)(2,1)S(1)} %bitcast.74, bf16[16,512,256]{2,1,0:T(8,128)(2,1)S(1)} %bitcast.73), custom_call_target="tpu_custom_call" | custom-call | flops 15000000512 | bytes 6000000 | tf_op jit(solution)/shard_map/flash/pallas_call | solution.py:102
  187.0 0.8 slice_bitcast_fusion
  187.7 1.5 collective-permute-start.9
  189.2 1.1 collective-permute-start.8
  190.3 2.4 collective-permute-start.7
  192.7 0.7 copy.57.gain_ref
  193.4 4.2 %collective-permute-done.9.three_ref = bf16[4,144,256]{2,1,0:T(8,128)(2,1)S(1)} collective-permute-done((bf16[4,144,256]{2,1,0:T(8,128)(2,1)S(1)}, bf16[4,144,256]{2,1,0:T(8,128)(2,1)S(1)}, u32[]{:S(2)}, u32[]{:S(2)}) %collective-permute-start.9) | collective-permute-done | bytes 294944 | tf_op jit(solution)/shard_map/ppermute | solution.py:161
  197.6 3.0 %collective-permute-done.8.two_ref = bf16[4,144,256]{2,1,0:T(8,128)(2,1)S(1)} collective-permute-done((bf16[4,144,256]{2,1,0:T(8,128)(2,1)S(1)}, bf16[4,144,256]{2,1,0:T(8,128)(2,1)S(1)}, u32[]{:S(2)}, u32[]{:S(2)}) %collective-permute-start.8) | collective-permute-done | bytes 294944 | tf_op jit(solution)/shard_map/ppermute | solution.py:161
  200.6 4.6 %collective-permute-done.7.one_ref = bf16[4,144,256]{2,1,0:T(8,128)(2,1)S(1)} collective-permute-done((bf16[4,144,256]{2,1,0:T(8,128)(2,1)S(1)}, bf16[4,144,256]{2,1,0:T(8,128)(2,1)S(1)}, u32[]{:S(2)}, u32[]{:S(2)}) %collective-permute-start.7) | collective-permute-done | bytes 294944 | tf_op jit(solution)/shard_map/ppermute | solution.py:161
  205.2 0.7 copy-done.4
  205.9 2.3 merge.1
  208.2 0.9 fusion.29
  209.1 2.3 collective-permute-start.10
  211.4 3.8 %collective-permute-done.10 = bf16[256,128]{1,0:T(8,128)(2,1)S(1)} collective-permute-done((bf16[256,128]{1,0:T(8,128)(2,1)S(1)}, bf16[256,128]{1,0:T(8,128)(2,1)S(1)}, u32[]{:S(2)}, u32[]{:S(2)}) %collective-permute-start.10) | collective-permute-done | bytes 65568 | tf_op jit(solution)/shard_map/ppermute | solution.py:161
  215.2 1.5 convolution_convert_fusion
  216.7 0.0 reduce-scatter.3.cloned.1.call-update
  216.7 0.0 reduce-scatter.5.cloned.1.call-done
  216.7 2.1 reshape.57
  218.8 8.9 %all-to-all-start.1 = ((bf16[64,10,512]{2,1,0:T(8,128)(2,1)}), bf16[64,10,512]{2,1,0:T(8,128)(2,1)S(1)}, u32[]{:S(2)}, u32[]{:S(2)}) async-start(bf16[64,10,512]{2,1,0:T(8,128)(2,1)} %reshape.57), calls=%async_computation.3 | async-start | bytes 2097152 | tf_op jit(solution)/shard_map/all_to_all | solution.py:231
  227.7 0.2 select_reduce_fusion
  227.9 28.6 %all-to-all-done.1 = bf16[64,10,512]{2,1,0:T(8,128)(2,1)S(1)} async-done(((bf16[64,10,512]{2,1,0:T(8,128)(2,1)}), bf16[64,10,512]{2,1,0:T(8,128)(2,1)S(1)}, u32[]{:S(2)}, u32[]{:S(2)}) %all-to-all-start.1) | async-done | bytes 655392 | tf_op jit(solution)/shard_map/all_to_all | solution.py:231
  256.5 0.2 reshape.58
  256.7 1.0 fusion.31
  (40 shorter events, 0.2 us)
Async XLA Ops:
  7.2 208.0 %copy-start = (bf16[256,2048]{1,0:T(8,128)(2,1)S(1)}, bf16[256,2048]{1,0:T(8,128)(2,1)}, u32[]{:S(2)}) copy-start(bf16[256,2048]{1,0:T(8,128)(2,1)} %param.18) | copy-start | bytes 3145732
  7.2 6.6 %copy-start.8 = (s32[192,2]{0,1:T(2,128)S(1)}, s32[192,2]{0,1:T(2,128)}, u32[]{:S(2)}) copy-start(s32[192,2]{0,1:T(2,128)} %param.21) | copy-start | bytes 4612
  7.2 85.5 %all-gather.4.cloned.1.call-start = ((), (), s32[]{:S(2)}) async-start(), calls=%async_computation.5 | async-start | bytes 3276800 | tf_op jit(solution)/shard_map/all_gather | solution.py:221
  16.4 41.9 %copy-start.6 = (bf16[256,256]{1,0:T(8,128)(2,1)S(1)}, bf16[256,256]{1,0:T(8,128)(2,1)}, u32[]{:S(2)}) copy-start(bf16[256,256]{1,0:T(8,128)(2,1)} %param.14) | copy-start | bytes 393220
  16.4 42.0 %copy-start.7 = (bf16[256,256]{1,0:T(8,128)(2,1)S(1)}, bf16[256,256]{1,0:T(8,128)(2,1)}, u32[]{:S(2)}) copy-start(bf16[256,256]{1,0:T(8,128)(2,1)} %param.15) | copy-start | bytes 393220
  58.2 88.3 %all-gather.6.cloned.1.call-start = ((), (), s32[]{:S(2)}) async-start(), calls=%async_computation.7 | async-start | bytes 4456448 | tf_op jit(solution)/shard_map/all_gather | solution.py:166
  59.2 157.6 %reduce-scatter.5.cloned.1.call-start = ((), (), s32[]{:S(2)}) async-start(), calls=%async_computation.6 | async-start | bytes 3276800 | tf_op jit(solution)/shard_map/reduce_scatter | solution.py:227
  114.1 0.9 copy-start.5
  114.1 143.6 %reduce-scatter.3.cloned.1.call-start = ((), (), s32[]{:S(2)}) async-start(), calls=%async_computation.4 | async-start | bytes 1310720 | tf_op jit(solution)/shard_map/reduce_scatter | solution.py:181
  115.0 13.3 %collective-permute-start.1 = (bf16[256,128]{0,1:T(8,128)(2,1)S(1)}, bf16[256,128]{0,1:T(8,128)(2,1)S(1)}, u32[]{:S(2)}, u32[]{:S(2)}) collective-permute-start(bf16[256,128]{0,1:T(8,128)(2,1)S(1)} %get-tuple-element.9), channel_id=1, source_target_pairs={{0,16},{8,24},{16,0},{24,8},{32,48},{40,56},{48,32},{56,40},{64,80... | collective-permute-start | bytes 196616 | tf_op jit(solution)/shard_map/ppermute | solution.py:161
  117.2 7.4 %collective-permute-start = (bf16[256,128]{0,1:T(8,128)(2,1)S(1)}, bf16[256,128]{0,1:T(8,128)(2,1)S(1)}, u32[]{:S(2)}, u32[]{:S(2)}) collective-permute-start(bf16[256,128]{0,1:T(8,128)(2,1)S(1)} %get-tuple-element.9), channel_id=1, source_target_pairs={{0,8},{8,16},{16,24},{24,0},{32,40},{40,48},{48,56},{56,32},{64,72... | collective-permute-start | bytes 196616 | tf_op jit(solution)/shard_map/ppermute | solution.py:161
  117.2 11.8 %collective-permute-start.2 = (bf16[256,128]{0,1:T(8,128)(2,1)S(1)}, bf16[256,128]{0,1:T(8,128)(2,1)S(1)}, u32[]{:S(2)}, u32[]{:S(2)}) collective-permute-start(bf16[256,128]{0,1:T(8,128)(2,1)S(1)} %get-tuple-element.9), channel_id=1, source_target_pairs={{0,24},{8,0},{16,8},{24,16},{32,56},{40,32},{48,40},{56,48},{64,88... | collective-permute-start | bytes 196616 | tf_op jit(solution)/shard_map/ppermute | solution.py:161
  119.2 22.8 %collective-permute-start.6 = (bf16[256,128]{0,1:T(8,128)(2,1)S(1)}, bf16[256,128]{0,1:T(8,128)(2,1)S(1)}, u32[]{:S(2)}, u32[]{:S(2)}) collective-permute-start(bf16[256,128]{0,1:T(8,128)(2,1)S(1)} %get-tuple-element.8), channel_id=1, source_target_pairs={{0,248},{8,224},{16,232},{24,240},{32,216},{40,192},{48,200},{56,2... | collective-permute-start | bytes 196616 | tf_op jit(solution)/shard_map/ppermute | solution.py:161
  124.6 17.3 %collective-permute-start.5 = (bf16[256,128]{0,1:T(8,128)(2,1)S(1)}, bf16[256,128]{0,1:T(8,128)(2,1)S(1)}, u32[]{:S(2)}, u32[]{:S(2)}) collective-permute-start(bf16[256,128]{0,1:T(8,128)(2,1)S(1)} %get-tuple-element.8), channel_id=1, source_target_pairs={{0,240},{8,248},{16,224},{24,232},{32,208},{40,216},{48,192},{56,2... | collective-permute-start | bytes 196616 | tf_op jit(solution)/shard_map/ppermute | solution.py:161
  124.6 17.3 %collective-permute-start.4 = (bf16[256,128]{0,1:T(8,128)(2,1)S(1)}, bf16[256,128]{0,1:T(8,128)(2,1)S(1)}, u32[]{:S(2)}, u32[]{:S(2)}) collective-permute-start(bf16[256,128]{0,1:T(8,128)(2,1)S(1)} %get-tuple-element.8), channel_id=1, source_target_pairs={{0,232},{8,240},{16,248},{24,224},{32,200},{40,208},{48,216},{56,1... | collective-permute-start | bytes 196616 | tf_op jit(solution)/shard_map/ppermute | solution.py:161
  128.3 13.6 %collective-permute-start.3 = (bf16[256,128]{0,1:T(8,128)(2,1)S(1)}, bf16[256,128]{0,1:T(8,128)(2,1)S(1)}, u32[]{:S(2)}, u32[]{:S(2)}) collective-permute-start(bf16[256,128]{0,1:T(8,128)(2,1)S(1)} %get-tuple-element.8), channel_id=1, source_target_pairs={{0,224},{8,232},{16,240},{24,248},{32,192},{40,200},{48,208},{56,2... | collective-permute-start | bytes 196616 | tf_op jit(solution)/shard_map/ppermute | solution.py:161
  152.9 2.2 copy-start.1
  155.1 37.6 %copy-start.10 = (f32[128]{0:T(128)S(1)}, f32[128]{0:T(128)}, u32[]{:S(2)}) copy-start(f32[128]{0:T(128)} %param.17) | copy-start | bytes 1540
  187.7 9.9 %collective-permute-start.9 = (bf16[4,144,256]{2,1,0:T(8,128)(2,1)S(1)}, bf16[4,144,256]{2,1,0:T(8,128)(2,1)S(1)}, u32[]{:S(2)}, u32[]{:S(2)}) collective-permute-start(bf16[4,144,256]{2,1,0:T(8,128)(2,1)S(1)} %get-tuple-element.2), channel_id=1, source_target_pairs={{0,8},{8,16},{16,24},{24,0},{32,40},{40,48},{48,56},{56,32},{64,72... | collective-permute-start | bytes 884744 | tf_op jit(solution)/shard_map/ppermute | solution.py:161
  189.2 11.4 %collective-permute-start.8 = (bf16[4,144,256]{2,1,0:T(8,128)(2,1)S(1)}, bf16[4,144,256]{2,1,0:T(8,128)(2,1)S(1)}, u32[]{:S(2)}, u32[]{:S(2)}) collective-permute-start(bf16[4,144,256]{2,1,0:T(8,128)(2,1)S(1)} %get-tuple-element.3), channel_id=1, source_target_pairs={{0,16},{8,24},{16,0},{24,8},{32,48},{40,56},{48,32},{56,40},{64,80... | collective-permute-start | bytes 884744 | tf_op jit(solution)/shard_map/ppermute | solution.py:161
  190.3 14.9 %collective-permute-start.7 = (bf16[4,144,256]{2,1,0:T(8,128)(2,1)S(1)}, bf16[4,144,256]{2,1,0:T(8,128)(2,1)S(1)}, u32[]{:S(2)}, u32[]{:S(2)}) collective-permute-start(bf16[4,144,256]{2,1,0:T(8,128)(2,1)S(1)} %get-tuple-element.4), channel_id=1, source_target_pairs={{0,24},{8,0},{16,8},{24,16},{32,56},{40,32},{48,40},{56,48},{64,88... | collective-permute-start | bytes 884744 | tf_op jit(solution)/shard_map/ppermute | solution.py:161
  197.6 7.6 %copy-start.2 = (bf16[4,144,256]{2,1,0:T(8,128)(2,1)}, bf16[4,144,256]{2,1,0:T(8,128)(2,1)S(1)}, u32[]{:S(2)}) copy-start(bf16[4,144,256]{2,1,0:T(8,128)(2,1)S(1)} %collective-permute-done.9.three_ref) | copy-start | bytes 884740
  200.6 4.6 %copy-start.3 = (bf16[4,144,256]{2,1,0:T(8,128)(2,1)}, bf16[4,144,256]{2,1,0:T(8,128)(2,1)S(1)}, u32[]{:S(2)}) copy-start(bf16[4,144,256]{2,1,0:T(8,128)(2,1)S(1)} %collective-permute-done.8.two_ref) | copy-start | bytes 884740
  205.2 0.7 copy-start.4
  209.1 6.1 %collective-permute-start.10 = (bf16[256,128]{1,0:T(8,128)(2,1)S(1)}, bf16[256,128]{1,0:T(8,128)(2,1)S(1)}, u32[]{:S(2)}, u32[]{:S(2)}) collective-permute-start(bf16[256,128]{1,0:T(8,128)(2,1)S(1)} %get-tuple-element.7), channel_id=1, source_target_pairs={{0,224},{8,232},{16,240},{24,248},{32,192},{40,200},{48,208},{56,2... | collective-permute-start | bytes 196616 | tf_op jit(solution)/shard_map/ppermute | solution.py:161
  216.7 11.1 %copy-start.9 = (f32[192,2]{0,1:T(2,128)S(1)}, f32[192,2]{0,1:T(2,128)}, u32[]{:S(2)}) copy-start(f32[192,2]{0,1:T(2,128)} %param.22) | copy-start | bytes 4612
  218.8 37.6 %all-to-all-start.1 = ((bf16[64,10,512]{2,1,0:T(8,128)(2,1)}), bf16[64,10,512]{2,1,0:T(8,128)(2,1)S(1)}, u32[]{:S(2)}, u32[]{:S(2)}) async-start(bf16[64,10,512]{2,1,0:T(8,128)(2,1)} %reshape.57), calls=%async_computation.3 | async-start | bytes 2097152 | tf_op jit(solution)/shard_map/all_to_all | solution.py:231
Sparse Core Ops, SparseCore 0:
  58.4 34.2 all-gather.3
  95.1 51.3 all-gather.5
  149.0 35.0 reduce-scatter.4
  216.8 25.6 reduce-scatter.2

commit v2 on v1

v2 whole, which is shorter than its diff:
```python
import functools
import math

import jax
import jax.numpy as jnp
from jax import lax
from jax.experimental import pallas as pl
from jax.experimental.pallas import tpu as pltpu
from jax.sharding import Mesh, PartitionSpec as P

EPS = 1e-06
NZ, NX, NC, NT = 8, 4, 2, 4
EP = ("z", "x", "core")
BLOCK = 256
HALF = BLOCK // 2
CHUNK = NC * BLOCK
COLS = 2 * NX * HALF
ACC = 144
COLS_T = 512
FULL, TAIL = 8, 2
NEAR = (0, 1, 7, 2, 6, 3, 5, 4)
PLUS = (0, 7, 6, 5)
LOW = -1e30
EXP2_SCALE = 64 ** (-0.5) * math.log2(math.e)


def pieces_of(value):
    first = value.astype(jnp.bfloat16).astype(jnp.float32)
    second = (value - first).astype(jnp.bfloat16).astype(jnp.float32)
    third = value - first - second
    return first, second, third


def flash_kernel(query_ref, pair_ref, out_ref, rhs_ref, max_ref, acc_ref):
    z, x, core = lax.axis_index("z"), lax.axis_index("x"), lax.axis_index("core")
    map_row = lax.broadcasted_iota(jnp.int32, (128, HALF), 0)
    ones = jnp.ones((ACC - 128, CHUNK), jnp.bfloat16)
    tile = 256

    for group in range(2):
        query_z = z if group == 0 else NZ - 1 - z
        for head in range(2):
            for step in range(NX):
                block = query_ref[group, step, head * 128 : (head + 1) * 128, :]
                for which in range(2):
                    first = (which * NX + step) * HALF
                    keep = (map_row < 64) if which == 0 else (map_row >= 64)
                    rhs_ref[:, first : first + HALF] = jnp.where(
                        keep, block, jnp.zeros_like(block)
                    )
            max_ref[...] = jnp.full_like(max_ref, LOW)
            acc_ref[...] = jnp.zeros_like(acc_ref)

            def work(step_z, masked):
                keys, values = [], []
                for c in range(NC):
                    keys.append(
                        pair_ref[step_z * NC + c, 0:256, head * 128 : (head + 1) * 128]
                    )
                    values.append(
                        pair_ref[step_z * NC + c, 256 + head * 128 : 256 + (head + 1) * 128, :]
                    )
                keys = jnp.concatenate(keys, axis=0)
                values = jnp.concatenate([jnp.concatenate(values, axis=1), ones], axis=0)
                for first in range(0, COLS, tile):
                    cols = slice(first, first + tile)
                    scores = jnp.dot(keys, rhs_ref[:, cols], preferred_element_type=jnp.float32)
                    if masked:
                        key = lax.broadcasted_iota(jnp.int32, (CHUNK, tile), 0)
                        key = key + 2 * BLOCK * x
                        col = lax.broadcasted_iota(jnp.int32, (CHUNK, tile), 1) + first
                        shift = (col // HALF) % NX
                        query_x = lax.rem(x - shift + NX, NX)
                        position = (2 * query_x + core) * BLOCK + group * HALF + col % HALF
                        scores = jnp.where(position >= key, scores, -3e38)
                    before = max_ref[0:1, cols]
                    now = jnp.maximum(before, jnp.max(scores, axis=0, keepdims=True))
                    weights = jnp.exp2((scores - now) * EXP2_SCALE).astype(jnp.bfloat16)
                    rescale = jnp.exp2((before - now) * EXP2_SCALE)
                    max_ref[0:1, cols] = now
                    acc_ref[:, cols] = acc_ref[:, cols] * rescale + jnp.dot(
                        values, weights, preferred_element_type=jnp.float32
                    )

            lax.fori_loop(0, query_z, lambda s, c: (work(s, False), c)[1], 0)
            work(query_z, True)

            row = lax.broadcasted_iota(jnp.int32, (ACC - 128, COLS), 0)
            stats = jnp.zeros((ACC - 128, COLS), jnp.float32)
            rows = pieces_of(acc_ref[128:129, :]) + pieces_of(max_ref[0:1, :])
            for index, piece in enumerate(rows):
                stats = jnp.where(row == index, piece, stats)
            for which in range(2):
                for step in range(NX):
                    first = (which * NX + step) * HALF
                    lanes = slice(group * HALF, (group + 1) * HALF)
                    out_ref[step, 2 * head + which, 0:128, lanes] = acc_ref[
                        0:128, first : first + HALF
                    ].astype(jnp.bfloat16)
                    out_ref[step, 2 * head + which, 128:ACC, lanes] = stats[
                        :, first : first + HALF
                    ].astype(jnp.bfloat16)


def flash(query_parts, pairs):
    return pl.pallas_call(
        flash_kernel,
        out_shape=jax.ShapeDtypeStruct((NX, 4, ACC, BLOCK), jnp.bfloat16),
        in_specs=[pl.BlockSpec(memory_space=pltpu.VMEM)] * 2,
        out_specs=pl.BlockSpec(memory_space=pltpu.VMEM),
        scratch_shapes=[
            pltpu.VMEM((128, COLS), jnp.bfloat16),
            pltpu.VMEM((8, COLS), jnp.float32),
            pltpu.VMEM((ACC, COLS), jnp.float32),
        ],
        compiler_params=pltpu.CompilerParams(vmem_limit_bytes=40 * 2**20),
        cost_estimate=pl.CostEstimate(
            flops=15_000_000_000, bytes_accessed=6_000_000, transcendentals=9_400_000
        ),
        name="flash",
    )(query_parts, pairs)


def places():
    return tuple(lax.axis_index(name) for name in (*EP, "tp"))


def remote(source, target, send, receive, device):
    return pltpu.make_async_remote_copy(
        src_ref=source,
        dst_ref=target,
        send_sem=send,
        recv_sem=receive,
        device_id=device,
        device_id_type=pl.DeviceIdType.MESH,
    )


def greet_all(z, x, c, t):
    me = (z * NX + x) * NC + c
    barrier = pltpu.get_barrier_semaphore()

    def signal(step, carry):
        peer = lax.rem(me + step, NZ * NX * NC)
        device = (peer // (NX * NC), lax.rem(peer // NC, NX), lax.rem(peer, NC), t)
        pl.semaphore_signal(
            barrier, inc=1, device_id=device, device_id_type=pl.DeviceIdType.MESH
        )
        return carry

    for dy in (1, NT - 1):
        pl.semaphore_signal(
            barrier,
            inc=1,
            device_id=(z, x, c, lax.rem(t + dy, NT)),
            device_id_type=pl.DeviceIdType.MESH,
        )
    lax.fori_loop(1, NZ * NX * NC, signal, 0)
    pl.semaphore_wait(barrier, NZ * NX * NC + 1)


def columns_of(t):
    return pl.ds(pl.multiple_of(t * COLS_T, COLS_T), COLS_T)


def dispatch_kernel(
    main_ref, tail_ref, pair_ref, query_ref, xmain, xtail, pairs, parts,
    own_sem, out_send, out_recv, y_send, y_recv, kv_send, kv_recv, c_send, c_recv, q_send, q_recv,
):
    z, x, c, t = places()
    me = (z * NX + x) * NC + c
    local = x * NC + c
    group = NX * NC
    after, before = lax.rem(t + 1, NT), lax.rem(t + NT - 1, NT)
    own = columns_of(t)
    own_copies = [
        pltpu.make_async_copy(main_ref.at[me], xmain.at[me, :, own], own_sem.at[0]),
        pltpu.make_async_copy(tail_ref.at[me], xtail.at[me, :, own], own_sem.at[1]),
        pltpu.make_async_copy(pair_ref, pairs.at[z * NC + c], own_sem.at[2]),
        pltpu.make_async_copy(query_ref.at[0], parts.at[0, 0], own_sem.at[3]),
    ]
    for copy in own_copies:
        copy.start()
    greet_all(z, x, c, t)

    for dz in (1, 7, 2, 6, 3, 5, 4, 0):
        to_z = lax.rem(z + dz, NZ)

        def send(step, carry):
            peer = lax.rem(local + step, group)
            device = (to_z, peer // NC, lax.rem(peer, NC), t)
            slab = to_z * group + peer
            for k, (source, target) in enumerate(((main_ref, xmain), (tail_ref, xtail))):
                remote(
                    source.at[slab], target.at[me, :, own],
                    out_send.at[k], out_recv.at[k, dz], device,
                ).start()
            return carry

        lax.fori_loop(1 if dz == 0 else 0, group, send, 0)

    mirrored = (NZ - 1 - z, x, c, t)
    remote(query_ref.at[1], parts.at[1, 0], q_send.at[3], q_recv.at[3], mirrored).start()
    for k in range(1, NX):
        device = (z, lax.rem(x + k, NX), c, t)
        remote(query_ref.at[0], parts.at[0, k], q_send.at[k - 1], q_recv.at[k - 1], device).start()

    up, down = (lax.rem(z + 1, NZ), x, c, t), (lax.rem(z + NZ - 1, NZ), x, c, t)
    across = (z, x, 1 - c, t)
    for way, device in enumerate((up, down)):
        remote(
            pair_ref, pairs.at[z * NC + c], kv_send.at[way, 0], kv_recv.at[way, 0], device
        ).start()
    remote(pair_ref, pairs.at[z * NC + c], c_send.at[0], c_recv.at[0], across).start()

    def rows_of(dz):
        return pl.ds(lax.rem(z - dz + NZ, NZ) * group, group)

    def y_copies(dz, slot, columns, device):
        rows = rows_of(dz)
        return [
            remote(
                target.at[rows, :, columns], target.at[rows, :, columns],
                y_send.at[slot, dz, k], y_recv.at[slot, dz, k], device,
            )
            for k, target in enumerate((xmain, xtail))
        ]

    to_after, to_before = (z, x, c, after), (z, x, c, before)

    def y_relay(dz):
        first = y_copies(dz, 0 if dz in PLUS else 1, own, to_after)
        for copy in first:
            copy.wait_recv()
        if dz in PLUS:
            copies = y_copies(dz, 2, columns_of(before), to_after)
        else:
            copies = y_copies(dz, 2, columns_of(after), to_before)
        for copy in copies:
            copy.start()

    def kv_step(step):
        for way, device in enumerate((up, down)):
            back = NZ - step if way == 0 else step
            block = lax.rem(z + back, NZ) * NC + c
            if step < 4:
                here = pairs.at[block]
                onward = here
                if step == 3:
                    onward = pairs.at[block, pl.ds(way * BLOCK, BLOCK), :]
            else:
                here = pairs.at[block, pl.ds(way * BLOCK, BLOCK), :]
            remote(
                here, here, kv_send.at[way, step - 1], kv_recv.at[way, step - 1], device
            ).wait_recv()
            if step < 4:
                remote(
                    onward, onward, kv_send.at[way, step], kv_recv.at[way, step], device
                ).start()
            slot = 2 * step - 1 + way
            remote(here, here, c_send.at[slot], c_recv.at[slot], across).start()

    for copy in own_copies:
        copy.wait()
    for index, dz in enumerate(NEAR):
        count = group - 1 if dz == 0 else group
        first = 0 if dz == 0 else lax.rem(z - dz + NZ, NZ) * group
        rows = pl.ds(first, count)
        for k, (source, target) in enumerate(((main_ref, xmain), (tail_ref, xtail))):
            remote(
                source.at[pl.ds(0, count)], target.at[rows, :, own],
                out_send.at[k], out_recv.at[k, dz], up,
            ).wait_recv()
        for slot, device in enumerate((to_after, to_before)):
            for copy in y_copies(dz, slot, own, device):
                copy.start()
        if index == 1:
            remote(
                query_ref.at[1], parts.at[1, 0], q_send.at[3], q_recv.at[3], mirrored
            ).wait_recv()
            for k in range(1, NX):
                device = (z, lax.rem(x + k, NX), c, t)
                remote(
                    parts.at[1, 0], parts.at[1, k], q_send.at[3 + k], q_recv.at[3 + k], device
                ).start()
        if index >= 2:
            y_relay(NEAR[index - 2])
    kv_step(1)
    y_relay(NEAR[6])
    y_relay(NEAR[7])
    for step in (2, 3, 4):
        kv_step(step)

    for dz in NEAR:
        for copy in y_copies(dz, 1 if dz in PLUS else 0, own, to_after):
            copy.wait_recv()
        for copy in y_copies(dz, 2, own, to_after):
            copy.wait_recv()
        for slot in range(3):
            for copy in y_copies(dz, slot, own, to_after):
                copy.wait_send()
    for k, (source, target) in enumerate(((main_ref, xmain), (tail_ref, xtail))):
        every = pl.ds(0, NZ * group - 1)
        remote(
            source.at[every], target.at[every, :, own], out_send.at[k], out_recv.at[k, 0], up
        ).wait_send()
    for way in range(2):
        for step in range(4):
            block = pairs.at[0] if step < 3 else pairs.at[0, pl.ds(0, BLOCK), :]
            remote(block, block, kv_send.at[way, step], kv_recv.at[way, step], up).wait_send()
    for slot in range(9):
        block = pairs.at[0] if slot < 7 else pairs.at[0, pl.ds(0, BLOCK), :]
        copy = remote(block, block, c_send.at[slot], c_recv.at[slot], across)
        copy.wait_send()
        copy.wait_recv()
    for slot in range(7):
        copy = remote(parts.at[0, 0], parts.at[0, 0], q_send.at[slot], q_recv.at[slot], up)
        copy.wait_send()
        if slot != 3:
            copy.wait_recv()


VMEM = pl.BlockSpec(memory_space=pltpu.VMEM)


def dispatch_call(main, tail, pair, queries):
    dma = pltpu.SemaphoreType.DMA
    slabs = NZ * NX * NC
    return pl.pallas_call(
        dispatch_kernel,
        out_shape=(
            jax.ShapeDtypeStruct((slabs, FULL, NT * COLS_T), jnp.bfloat16),
            jax.ShapeDtypeStruct((slabs, TAIL, NT * COLS_T), jnp.bfloat16),
            jax.ShapeDtypeStruct((NZ * NC, 2 * BLOCK, BLOCK), jnp.bfloat16),
            jax.ShapeDtypeStruct((2, NX, BLOCK, HALF), jnp.bfloat16),
        ),
        in_specs=[VMEM] * 4,
        out_specs=(VMEM,) * 4,
        scratch_shapes=[
            dma((4,)), dma((2,)), dma((2, NZ)), dma((3, NZ, 2)), dma((3, NZ, 2)),
            dma((2, 4)), dma((2, 4)), dma((9,)), dma((9,)), dma((7,)), dma((7,)),
        ],
        compiler_params=pltpu.CompilerParams(
            collective_id=0, has_side_effects=True, vmem_limit_bytes=24 * 2**20
        ),
        name="dispatch",
    )(main, tail, pair, queries)


def return_kernel(
    fmain, ftail, partial, rmain, rtail, parts,
    relay_main, relay_tail, sum_main, sum_tail, in_main, in_tail, red_main, red_tail,
    own_sem, p_send, p_recv, relay_send, relay_recv, y_send, y_recv, out_send, out_recv,
):
    z, x, c, t = places()
    me = (z * NX + x) * NC + c
    local = x * NC + c
    group = NX * NC
    after, before = lax.rem(t + 1, NT), lax.rem(t + NT - 1, NT)
    opposite = lax.rem(t + 2, NT)
    to_after, to_before = (z, x, c, after), (z, x, c, before)
    greet_all(z, x, c, t)
    far = NEAR[::-1]
    pairs = (
        (fmain, relay_main, sum_main, in_main, red_main, rmain),
        (ftail, relay_tail, sum_tail, in_tail, red_tail, rtail),
    )

    def rows_of(dz):
        return pl.ds(lax.rem(z + dz, NZ) * group, group)

    def relay_copy(dz, k):
        source, target = pairs[k][0], pairs[k][1]
        return remote(
            source.at[rows_of(dz), :, columns_of(opposite)], target.at[dz],
            relay_send.at[dz, k], relay_recv.at[dz, k],
            to_after if dz in PLUS else to_before,
        )

    def y_copy(dz, k, way, source):
        return remote(
            source, pairs[k][3].at[way, dz], y_send.at[way, dz, k], y_recv.at[way, dz, k],
            (to_after, to_before)[way],
        )

    def direct(dz, k):
        way = 1 if dz in PLUS else 0
        columns = columns_of((after, before)[way])
        return y_copy(dz, k, way, pairs[k][0].at[rows_of(dz), :, columns])

    for dz in far:
        for k in range(2):
            relay_copy(dz, k).start()
    for k in range(1, NX):
        device = (z, lax.rem(x + NX - k, NX), c, t)
        remote(partial.at[k], parts.at[k - 1], p_send.at[k - 1], p_recv.at[k - 1], device).start()
    for dz in far:
        for k in range(2):
            direct(dz, k).start()

    def add_relay(dz):
        way = 0 if dz in PLUS else 1
        columns = columns_of((after, before)[way])
        for k in range(2):
            relay_copy(dz, k).wait_recv()
            source, relayed, total = pairs[k][:3]
            mine = source[rows_of(dz), :, columns].astype(jnp.float32)
            total[dz] = (mine + relayed[dz].astype(jnp.float32)).astype(jnp.bfloat16)
            y_copy(dz, k, way, total.at[dz]).start()

    def finish(dz):
        to_z = lax.rem(z + dz, NZ)
        for k in range(2):
            source, arrived, reduced = pairs[k][0], pairs[k][3], pairs[k][4]
            for way in range(2):
                y_copy(dz, k, way, pairs[k][2].at[dz]).wait_recv()
            reduced[rows_of(dz)] = (
                source[rows_of(dz), :, columns_of(t)].astype(jnp.float32)
                + arrived[0, dz].astype(jnp.float32)
                + arrived[1, dz].astype(jnp.float32)
            ).astype(jnp.bfloat16)

        def send(step, carry):
            peer = lax.rem(local + step, group)
            device = (to_z, peer // NC, lax.rem(peer, NC), t)
            for k in range(2):
                remote(
                    pairs[k][4].at[to_z * group + peer], pairs[k][5].at[me],
                    out_send.at[k], out_recv.at[k], device,
                ).start()
            return carry

        lax.fori_loop(1 if dz == 0 else 0, group, send, 0)
        if dz == 0:
            for k in range(2):
                pltpu.make_async_copy(
                    pairs[k][4].at[me], pairs[k][5].at[me], own_sem.at[k]
                ).start()

    for index, dz in enumerate(far):
        add_relay(dz)
        if index >= 1:
            finish(far[index - 1])
    finish(far[-1])

    for k in range(2):
        pltpu.make_async_copy(pairs[k][4].at[me], pairs[k][5].at[me], own_sem.at[k]).wait()
        every = pl.ds(0, NZ * group - 1)
        copy = remote(
            pairs[k][4].at[every], pairs[k][5].at[every], out_send.at[k], out_recv.at[k], to_after
        )
        copy.wait_recv()
        copy.wait_send()
        for dz in far:
            relay_copy(dz, k).wait_send()
            for way in range(2):
                y_copy(dz, k, way, pairs[k][2].at[dz]).wait_send()
    for k in range(1, NX):
        copy = remote(partial.at[k], parts.at[k - 1], p_send.at[k - 1], p_recv.at[k - 1], to_after)
        copy.wait_recv()
        copy.wait_send()


def return_call(fmain, ftail, partial):
    dma = pltpu.SemaphoreType.DMA
    slabs = NZ * NX * NC
    group = NX * NC

    def both(*lead):
        return [
            pltpu.VMEM((*lead, rows, COLS_T), jnp.bfloat16) for rows in (FULL, TAIL)
        ]

    return pl.pallas_call(
        return_kernel,
        out_shape=(
            jax.ShapeDtypeStruct((slabs, FULL, COLS_T), jnp.bfloat16),
            jax.ShapeDtypeStruct((slabs, TAIL, COLS_T), jnp.bfloat16),
            jax.ShapeDtypeStruct((NX - 1, 4, ACC, BLOCK), jnp.bfloat16),
        ),
        in_specs=[VMEM] * 3,
        out_specs=(VMEM,) * 3,
        scratch_shapes=[
            *both(NZ, group), *both(NZ, group), *both(2, NZ, group), *both(slabs),
            dma((2,)), dma((3,)), dma((3,)), dma((NZ, 2)), dma((NZ, 2)),
            dma((2, NZ, 2)), dma((2, NZ, 2)), dma((2,)), dma((2,)),
        ],
        compiler_params=pltpu.CompilerParams(
            collective_id=1, has_side_effects=True, vmem_limit_bytes=24 * 2**20
        ),
        name="give_back",
    )(fmain, ftail, partial)


def hidden_kernel(xmain, xtail, gate, up, down, fmain, ftail, rows, hidden):
    count = xmain.shape[0]
    rows[0:count] = xmain[...]
    rows[count:] = xtail[...]
    width = gate.shape[1]
    for first in range(0, width, 256):
        cols = slice(first, min(first + 256, width))
        gate_act = jnp.dot(rows[...], gate[:, cols], preferred_element_type=jnp.float32)
        up_act = jnp.dot(rows[...], up[:, cols], preferred_element_type=jnp.float32)
        value = gate_act / (1.0 + jnp.exp(-gate_act)) * up_act
        hidden[:, cols] = value.astype(jnp.bfloat16)
    for first in range(0, fmain.shape[1], 256):
        cols = slice(first, first + 256)
        out = jnp.dot(hidden[...], down[:, cols], preferred_element_type=jnp.float32)
        fmain[:, cols] = out[0:count].astype(jnp.bfloat16)
        ftail[:, cols] = out[count:].astype(jnp.bfloat16)


def hidden_call(xmain, xtail, gate, up, down):
    return pl.pallas_call(
        hidden_kernel,
        out_shape=(
            jax.ShapeDtypeStruct(xmain.shape, jnp.bfloat16),
            jax.ShapeDtypeStruct(xtail.shape, jnp.bfloat16),
        ),
        in_specs=[VMEM] * 5,
        out_specs=(VMEM,) * 2,
        scratch_shapes=[
            pltpu.VMEM((xmain.shape[0] + xtail.shape[0], xmain.shape[1]), jnp.bfloat16),
            pltpu.VMEM((xmain.shape[0] + xtail.shape[0], gate.shape[1]), jnp.bfloat16),
        ],
        compiler_params=pltpu.CompilerParams(vmem_limit_bytes=32 * 2**20),
        cost_estimate=pl.CostEstimate(
            flops=7_000_000_000, bytes_accessed=16_000_000, transcendentals=600_000
        ),
        name="hidden",
    )(xmain, xtail, gate, up, down)


def mixer_kernel(
    lambda_ref, gain_ref, partial_ref, parts_ref, weight_ref, out_ref,
    attended, upper_send, upper_recv, blocks, relayed, totals, arrived,
    u_send, u_recv, relay_send, relay_recv, y_send, y_recv,
):
    z, x, c, t = places()
    after, before = lax.rem(t + 1, NT), lax.rem(t + NT - 1, NT)
    opposite = lax.rem(t + 2, NT)
    devices = ((z, x, c, after), (z, x, c, before))
    mirrored = (NZ - 1 - z, x, c, t)
    barrier = pltpu.get_barrier_semaphore()
    for device in (*devices, mirrored):
        pl.semaphore_signal(
            barrier, inc=1, device_id=device, device_id_type=pl.DeviceIdType.MESH
        )

    for head in range(2):
        per_map = []
        for which in range(2):
            index = 2 * head + which
            sources = [partial_ref.at[0, index]] + [parts_ref.at[k, index] for k in range(NX - 1)]
            totals_of, maxima = [], []
            for part in sources:
                stats = part[128:ACC, :].astype(jnp.float32)
                totals_of.append(stats[0:1] + stats[1:2] + stats[2:3])
                maxima.append(stats[3:4] + stats[4:5] + stats[5:6])
            largest = functools.reduce(jnp.maximum, maxima)
            total, numerator = 0.0, 0.0
            for part, own_total, own_max in zip(sources, totals_of, maxima):
                factor = jnp.exp2((own_max - largest) * EXP2_SCALE)
                total = total + factor * own_total
                numerator = numerator + factor * part[0:128, :].astype(jnp.float32)
            per_map.append(numerator / total)
        contrast = per_map[0] - lambda_ref[head] * per_map[1]
        square = jnp.mean(contrast * contrast, axis=0, keepdims=True)
        normed = contrast * lax.rsqrt(square + EPS) * gain_ref[...]
        normed = normed.astype(jnp.bfloat16)
        attended[head * 128 : (head + 1) * 128, :] = normed[:, :HALF]
        upper_send[head * 128 : (head + 1) * 128, :] = normed[:, HALF:]

    pl.semaphore_wait(barrier, 3)
    flip = remote(upper_send, upper_recv, u_send, u_recv, mirrored)
    flip.start()
    rows = BLOCK // NT
    half = rows // 2

    def project(source, first):
        for low in range(0, 2048, 512):
            part = lax.dot_general(
                source[...], weight_ref[:, low : low + 512],
                (((0,), (0,)), ((), ())), preferred_element_type=jnp.float32,
            ).astype(jnp.bfloat16)
            blocks[first, :, low : low + 512] = part[:rows]
            blocks[first + 1, :, low : low + 512] = part[rows:]

    project(attended, 0)
    flip.wait()
    project(upper_recv, 2)

    def relay_copy(way):
        return remote(
            blocks.at[opposite, pl.ds(way * half, half), :], relayed.at[way],
            relay_send.at[way], relay_recv.at[way], devices[way],
        )

    def y_copy(way, part, source):
        return remote(
            source, arrived.at[way, pl.ds(part * half, half), :],
            y_send.at[way, part], y_recv.at[way, part], devices[way],
        )

    for way in range(2):
        relay_copy(way).start()
    for way in range(2):
        source = blocks.at[(after, before)[way], pl.ds((1 - way) * half, half), :]
        y_copy(way, 1 - way, source).start()
    for way in range(2):
        relay_copy(way).wait_recv()
        mine = blocks[(after, before)[way], way * half : (way + 1) * half, :]
        totals[way] = (
            mine.astype(jnp.float32) + relayed[way].astype(jnp.float32)
        ).astype(jnp.bfloat16)
        y_copy(way, way, totals.at[way]).start()
    for way in range(2):
        for part in range(2):
            copy = y_copy(way, part, totals.at[way])
            copy.wait_recv()
            copy.wait_send()
        relay_copy(way).wait_send()
    out_ref[...] = (
        blocks[t].astype(jnp.float32)
        + arrived[0].astype(jnp.float32)
        + arrived[1].astype(jnp.float32)
    ).astype(jnp.bfloat16)


def mixer_call(head_lambda, sub_gain, partial, parts, out_weight):
    dma = pltpu.SemaphoreType.DMA
    rows, width = BLOCK // NT, out_weight.shape[1]
    return pl.pallas_call(
        mixer_kernel,
        out_shape=jax.ShapeDtypeStruct((rows, width), jnp.bfloat16),
        in_specs=[pl.BlockSpec(memory_space=pltpu.SMEM)] + [VMEM] * 4,
        out_specs=VMEM,
        scratch_shapes=[
            pltpu.VMEM((BLOCK, HALF), jnp.bfloat16),
            pltpu.VMEM((BLOCK, HALF), jnp.bfloat16),
            pltpu.VMEM((BLOCK, HALF), jnp.bfloat16),
            pltpu.VMEM((NT, rows, width), jnp.bfloat16),
            pltpu.VMEM((2, rows // 2, width), jnp.bfloat16),
            pltpu.VMEM((2, rows // 2, width), jnp.bfloat16),
            pltpu.VMEM((2, rows, width), jnp.bfloat16),
            dma(()), dma(()), dma((2,)), dma((2,)), dma((2, 2)), dma((2, 2)),
        ],
        compiler_params=pltpu.CompilerParams(
            collective_id=2, has_side_effects=True, vmem_limit_bytes=24 * 2**20
        ),
        name="mixer",
    )(head_lambda, sub_gain[:, None], partial, parts, out_weight)


def shards(
    queries,
    key_rows,
    value_rows,
    head_lambda,
    sub_gain,
    out_weight,
    expert_input,
    norm_gain,
    route_ids,
    route_weight,
    gate_weight,
    up_weight,
    down_weight,
):
    rows_here, model_width = expert_input.shape
    experts = NZ * NX * NC
    top_count = route_ids.shape[1]
    slots = experts * (FULL + TAIL)
    wide_rows = expert_input.astype(jnp.float32)
    normed = (
        wide_rows
        * lax.rsqrt(jnp.mean(wide_rows * wide_rows, axis=-1, keepdims=True) + EPS)
        * norm_gain
    ).astype(jnp.bfloat16)
    flat_ids = route_ids.reshape(-1)
    onehot = (flat_ids[:, None] == jnp.arange(experts, dtype=jnp.int32)[None, :]).astype(jnp.int32)
    rank_before = jnp.cumsum(onehot, axis=0) - onehot
    slot = jnp.sum(rank_before * onehot, axis=1)
    buffer_pos = jnp.where(
        slot < FULL,
        flat_ids * FULL + slot,
        experts * FULL + flat_ids * TAIL + slot - FULL,
    ).reshape(rows_here, top_count)
    matches = buffer_pos[None, :, :] == jnp.arange(slots, dtype=jnp.int32)[:, None, None]
    dispatch = jnp.any(matches, axis=-1).astype(jnp.bfloat16)
    combine = jnp.sum(jnp.where(matches, route_weight[None, :, :], 0.0), axis=-1)
    own_cols = lax.dynamic_slice_in_dim(normed, lax.axis_index("tp") * COLS_T, COLS_T, 1)
    outgoing = jnp.dot(dispatch, own_cols, preferred_element_type=jnp.float32).astype(jnp.bfloat16)
    main = outgoing[: experts * FULL].reshape(experts, FULL, COLS_T)
    tail = outgoing[experts * FULL :].reshape(experts, TAIL, COLS_T)
    pair = jnp.concatenate([key_rows, value_rows.T], axis=0)
    turned = queries.T
    halves = jnp.stack([turned[:, :HALF], turned[:, HALF:]])

    xmain, xtail, pairs, parts = dispatch_call(main, tail, pair, halves)
    fmain, ftail = hidden_call(
        xmain.reshape(experts * FULL, model_width),
        xtail.reshape(experts * TAIL, model_width),
        gate_weight[0],
        up_weight[0],
        down_weight[0],
    )
    partial = flash(parts, pairs)
    rmain, rtail, others = return_call(
        fmain.reshape(experts, FULL, model_width),
        ftail.reshape(experts, TAIL, model_width),
        partial,
    )
    mixer_out = mixer_call(head_lambda, sub_gain, partial, others, out_weight)
    returned = jnp.concatenate(
        [rmain.reshape(experts * FULL, COLS_T), rtail.reshape(experts * TAIL, COLS_T)], axis=0
    )
    mixed = lax.dot_general(
        combine,
        returned.astype(jnp.float32),
        (((0,), (0,)), ((), ())),
        preferred_element_type=jnp.float32,
    )
    return (mixer_out, mixed.astype(jnp.bfloat16))


def solution(mesh):
    mesh = Mesh(mesh.devices.reshape(NZ, NX, NC, NT), (*EP, "tp"))
    placed = (
        P(EP, "tp"),
        P(EP, "tp"),
        P(EP, "tp"),
        P("tp"),
        P(),
        P("tp", None),
        P(EP, None),
        P(),
        P(EP, None),
        P(EP, None),
        P(EP, None, "tp"),
        P(EP, None, "tp"),
        P(EP, "tp", None),
    )
    return jax.shard_map(
        shards,
        mesh=mesh,
        in_specs=placed,
        out_specs=(P((*EP, "tp"), None), P(EP, "tp")),
        check_vma=False,
    )
```

time: 265 us -> 190 us (0.72)
  Pallas kernels: 34.2 us -> 162 us
  waiting for transfers between devices: 94.9 us -> 0 us
  blocking collectives: 40.7 us -> 0 us
  starting transfers between devices: 30.2 us -> 0 us
  matrix products: 20.9 us -> 2.49 us
  between operations: 14 us -> 0.9 us
  local copies, waits for them, and re-layouts: 23.4 us -> 19.6 us
  other arithmetic: 6.01 us -> 2.56 us
    pallas_call x1 -> x4, Pallas kernels: 2.29 us -> 130 us  [the longest x1 62.7 us: dispatch_call(): pl.pallas_call(dispatch_kernel, out_shape=(jax.ShapeDtypeStruct((slabs, F...]
    all_to_all x1 -> x0, blocking collectives: 40.7 us -> none  [expert_half(): lax.all_to_all(outgoing.reshape(experts, capacity, column_share), EP, spl...]
    all_gather x2 -> x0, waiting for transfers between devices: 37.7 us -> none  [the longest x1 33.5 us: expert_half(): pieces = lax.all_gather(arrived, 'tp', axis=0, tiled=False)]
    ppermute x11 -> x0, waiting for transfers between devices: 28.6 us -> none  [moved(): return lax.ppermute(array, ('z', 'x'), pairs)]
    all_to_all x1 -> x0, waiting for transfers between devices: 28.6 us -> none  [expert_half(): lax.all_to_all(summed.reshape(experts, capacity, col_count), EP, split_ax...]
    ppermute x11 -> x0, starting transfers between devices: 21.1 us -> none  [moved(): return lax.ppermute(array, ('z', 'x'), pairs)]
    dot_general x5 -> x2, matrix products: 20.9 us -> 2.49 us  [the longest x1 2.04 us: shards(): lax.dot_general(combine, returned.astype(jnp.float32), (((0,), (0,)), (()...]
    all_gather x2 -> x0, local copies, waits for them, and re-layouts: 10.8 us -> none  [the longest x1 6.38 us: mixer_half(): pairs = lax.all_gather(pair, ('z', 'core'), axis=0, tiled=False)]
  transfers between devices with their start and end apart: 16 -> 0, of which waited for: 8 -> 0; matrix products, arithmetic and copies ran while one was open for 14% -> 0% of each run, Pallas kernels for 13% -> 0%
where the time goes in v2:
time: 190 us; the launch traced here: 187 us
  Pallas kernels  162 us (85%)
  local copies, waits for them, and re-layouts  19.6 us (10%)
  other arithmetic  2.56 us (1%)
  matrix products  2.49 us (1%)
    pallas_call x1, Pallas kernels, dispatch_call(): pl.pallas_call(dispatch_kernel, out_shape=(jax.ShapeDtypeStruct((slabs, F...  62.7 us
    pallas_call x1, Pallas kernels, return_call(): pl.pallas_call(return_kernel, out_shape=(jax.ShapeDtypeStruct((slabs, FUL...  42.1 us
    pallas_call x1, Pallas kernels, flash(): pl.pallas_call(flash_kernel, out_shape=jax.ShapeDtypeStruct((NX, 4, ACC,...  31.8 us
    pallas_call x1, Pallas kernels, mixer_call(): pl.pallas_call(mixer_kernel, out_shape=jax.ShapeDtypeStruct((rows, width)...  16.7 us
    unnamed x36, local copies, waits for them, and re-layouts  13.9 us
    pallas_call x1, Pallas kernels, hidden_call(): pl.pallas_call(hidden_kernel, out_shape=(jax.ShapeDtypeStruct(xmain.shape...  8.28 us

profile of v2, /device:TPU:2, one launch (start us, length us, event | category | flops | bytes accessed | tf_op | source)
XLA Modules:
  0.0 187.2 jit_solution(16317401168909564621)
XLA Ops:
  0.6 0.0 copy-start.11
  0.6 0.8 copy.52.gain_ref
  1.5 0.8 copy.44
  2.3 0.1 eq.38
  2.4 0.1 eq.42
  2.6 0.9 reduce-window.6
  3.5 0.2 slice_reduce_fusion
  3.8 0.1 fusion.11
  3.9 0.1 reduce_sum.30
  4.0 0.1 copy.47
  4.1 0.7 compare_select_fusion
  4.8 0.1 fusion
  5.0 0.0 copy-done.11
  5.0 0.2 convert_element_type.23
  5.1 0.8 dynamic-slice
  5.9 0.0 copy-start.12
  5.9 0.2 multiply_reduce_fusion
  6.2 0.0 copy-start.14
  6.2 0.0 copy-start.13
  6.2 0.4 convolution_convert_fusion
  6.7 0.1 reshape.72.tail_ref
  6.8 0.1 copy-done.12
  6.8 0.1 copy.50
  6.9 0.2 copy-done.14
  7.1 0.0 copy-done.13
  7.1 0.1 copy.51
  7.3 62.7 %dispatch.1 = (bf16[64,8,2048]{2,1,0:T(8,128)(2,1)S(1)}, bf16[64,2,2048]{2,1,0:T(2,128)(2,1)S(1)}, bf16[16,512,256]{2,1,0:T(8,128)(2,1)S(1)}, bf16[2,4,256,128]{3,2,1,0:T(8,128)(2,1)S(1)}) custom-call(bf16[64,8,512]{2,1,0:T(8,128)(2,1)S(1)} %slice_bitcast_fusion.main_ref, bf16[64,2,512]{2,1,0:T(2,128)(2,1)S(1)} %reshape.72.tail_ref, ...), custom_call_target="tpu_custom_call" | custom-call | tf_op jit(solution)/shard_map/dispatch/pallas_call | solution.py:329
  70.0 0.0 copy-start.8
  70.0 1.3 copy-done.8
  71.4 31.8 %flash.1.partial.partial_ref = bf16[4,4,144,256]{3,2,1,0:T(8,128)(2,1)S(1)} custom-call(bf16[2,4,256,128]{3,2,1,0:T(8,128)(2,1)S(1)} %get-tuple-element.11.query_ref, bf16[16,512,256]{2,1,0:T(8,128)(2,1)S(1)} %get-tuple-element.12.pair_ref), custom_call_target="tpu_custom_call" | custom-call | flops 15000000512 | bytes 6000000 | tf_op jit(solution)/shard_map/flash/pallas_call | solution.py:106
  103.2 1.0 reshape.74.xtail
  104.2 0.0 copy-start.2
  104.2 1.0 copy-done.2
  105.3 0.0 copy-start.5
  105.3 2.0 %copy-done.5 = bf16[1,2048,896]{2,1,0:T(8,128)(2,1)S(1)} copy-done((bf16[1,2048,896]{2,1,0:T(8,128)(2,1)S(1)}, bf16[1,2048,896]{2,1,0:T(8,128)(2,1)}, u32[]{:S(2)}) %copy-start.5) | copy-done | bytes 3670040
  107.3 0.0 copy-start.6
  107.3 2.0 %copy-done.6 = bf16[1,2048,896]{2,1,0:T(8,128)(2,1)S(1)} copy-done((bf16[1,2048,896]{2,1,0:T(8,128)(2,1)S(1)}, bf16[1,2048,896]{2,1,0:T(8,128)(2,1)}, u32[]{:S(2)}) %copy-start.6) | copy-done | bytes 3670040
  109.3 0.0 copy-start.7
  109.3 2.0 %copy-done.7 = bf16[1,896,2048]{2,1,0:T(8,128)(2,1)S(1)} copy-done((bf16[1,896,2048]{2,1,0:T(8,128)(2,1)S(1)}, bf16[1,896,2048]{2,1,0:T(8,128)(2,1)}, u32[]{:S(2)}) %copy-start.7) | copy-done | bytes 3670040
  111.4 0.0 copy-start.9
  111.4 1.6 copy-done.9
  113.0 8.3 %hidden.1 = (bf16[512,2048]{1,0:T(8,128)(2,1)S(1)}, bf16[128,2048]{1,0:T(8,128)(2,1)S(1)}) custom-call(bf16[512,2048]{1,0:T(8,128)(2,1)S(1)} %bitcast.41, bf16[128,2048]{1,0:T(8,128)(2,1)S(1)} %copy-done.2, bf16[2048,896]{1,0:T(8,128)(2,1)S(1)} %bitcast.38, bf16[2048,896]{1,0:T(8,128)(2,1)S(1)} %bitcast.39, bf16[896,2048]{1,0:T(8,128)(2,1)S(1)} %bitcast.40), custom_call_target="tpu_custom_call" | custom-call | flops 7000000000 | bytes 16000000 | tf_op jit(solution)/shard_map/hidden/pallas_call | solution.py:514
  121.3 0.0 copy-start.3
  121.3 0.8 copy-done.3
  122.0 2.2 %reshape.76.ftail = bf16[64,2,2048]{2,1,0:T(2,128)(2,1)} reshape(bf16[128,2048]{1,0:T(8,128)(2,1)} %copy-done.3) | data formatting | bytes 1048576 | tf_op jit(solution)/shard_map/reshape | solution.py:711
  124.2 0.0 copy-start
  124.2 1.0 copy-done
  125.3 0.0 copy-start.1
  125.3 0.0 copy-start.4
  125.3 42.1 %give_back.1 = (bf16[64,8,512]{2,1,0:T(8,128)(2,1)S(1)}, bf16[64,2,512]{2,1,0:T(2,128)(2,1)S(1)}, bf16[3,4,144,256]{3,2,1,0:T(8,128)(2,1)S(1)}) custom-call(bf16[64,8,2048]{2,1,0:T(8,128)(2,1)S(1)} %bitcast.37, bf16[64,2,2048]{2,1,0:T(2,128)(2,1)S(1)} %copy-done, bf16[4,4,144,256]{3,2,1,0:T(8,128)(2,1)S(1)} %flash.1.partial.partial_ref), custom_call_target="tpu_custom_call" | custom-call | tf_op jit(solution)/shard_map/give_back/pallas_call | solution.py:474
  167.4 0.0 copy-start.10
  167.4 0.0 copy-done.1
  167.5 0.0 copy-done.4
  167.5 0.0 copy-start.15
  167.5 16.7 %mixer.1 = bf16[64,2048]{1,0:T(8,128)(2,1)S(1)} custom-call(f32[2]{0:T(128)S(1)} %copy-done.4, f32[128,1]{1,0:T(8,128)S(1)} %copy.52.gain_ref, bf16[4,4,144,256]{3,2,1,0:T(8,128)(2,1)S(1)} %flash.1.partial.partial_ref, bf16[3,4,144,256]{3,2,1,0:T(8,128)(2,1)S(1)} %get-tuple-element.17.parts_ref, bf16[256,2048]{1,0:T(8,128)(2,1)S(1)} %copy-done.1), custom_call_target="tpu_custom_call" | custom-call | tf_op jit(solution)/shard_map/mixer/pallas_call | solution.py:633
  184.2 0.0 copy-done.10
  184.2 0.0 copy-done.15
  184.2 0.2 select_reduce_fusion
  184.4 0.1 reshape.78
  184.4 2.0 %convolution_convert_fusion.1 = bf16[192,512]{1,0:T(8,128)(2,1)} fusion(bf16[640,192]{0,1:T(8,128)(2,1)S(1)} %select_reduce_fusion, bf16[128,512]{1,0:T(8,128)(2,1)S(1)} %reshape.78, bf16[512,512]{1,0:T(8,128)(2,1)} %bitcast.42), kind=kOutput, calls=%fused_computation.2 | convolution fusion | flops 127139840 | bytes 1097728 | tf_op jit(solution)/shard_map/dot_general | solution.py:718
  186.5 0.7 copy.56
  (8 shorter events, 0.1 us)
Async XLA Ops:
  0.6 4.3 %copy-start.11 = (bf16[192,2048]{1,0:T(8,128)(2,1)S(1)}, bf16[192,2048]{1,0:T(8,128)(2,1)}, u32[]{:S(2)}) copy-start(bf16[192,2048]{1,0:T(8,128)(2,1)} %param.19) | copy-start | bytes 2359300
  5.9 0.9 copy-start.12
  6.2 0.9 copy-start.14
  6.2 1.0 copy-start.13
  70.0 1.4 copy-start.8
  104.2 1.0 copy-start.2
  105.3 2.0 %copy-start.5 = (bf16[1,2048,896]{2,1,0:T(8,128)(2,1)S(1)}, bf16[1,2048,896]{2,1,0:T(8,128)(2,1)}, u32[]{:S(2)}) copy-start(bf16[1,2048,896]{2,1,0:T(8,128)(2,1)} %param.23) | copy-start | bytes 11010052
  107.3 2.0 %copy-start.6 = (bf16[1,2048,896]{2,1,0:T(8,128)(2,1)S(1)}, bf16[1,2048,896]{2,1,0:T(8,128)(2,1)}, u32[]{:S(2)}) copy-start(bf16[1,2048,896]{2,1,0:T(8,128)(2,1)} %param.24) | copy-start | bytes 11010052
  109.3 2.0 %copy-start.7 = (bf16[1,896,2048]{2,1,0:T(8,128)(2,1)S(1)}, bf16[1,896,2048]{2,1,0:T(8,128)(2,1)}, u32[]{:S(2)}) copy-start(bf16[1,896,2048]{2,1,0:T(8,128)(2,1)} %param.25) | copy-start | bytes 11010052
  111.4 1.6 copy-start.9
  121.3 0.8 copy-start.3
  124.2 1.0 copy-start
  125.3 42.2 %copy-start.1 = (bf16[256,2048]{1,0:T(8,128)(2,1)S(1)}, bf16[256,2048]{1,0:T(8,128)(2,1)}, u32[]{:S(2)}) copy-start(bf16[256,2048]{1,0:T(8,128)(2,1)} %weight_ref.1) | copy-start | bytes 3145732
  125.3 42.2 %copy-start.4 = (f32[2]{0:T(128)S(1)}, f32[2]{0:T(128)}, u32[]{:S(2)}) copy-start(f32[2]{0:T(128)} %lambda_ref.1) | copy-start | bytes 28
  167.4 16.7 %copy-start.10 = (bf16[64,8,512]{2,1,0:T(8,128)(2,1)}, bf16[64,8,512]{2,1,0:T(8,128)(2,1)S(1)}, u32[]{:S(2)}) copy-start(bf16[64,8,512]{2,1,0:T(8,128)(2,1)S(1)} %get-tuple-element.18) | copy-start | bytes 1572868
  167.5 16.7 %copy-start.15 = (f32[192,2]{0,1:T(2,128)S(1)}, f32[192,2]{0,1:T(2,128)}, u32[]{:S(2)}) copy-start(f32[192,2]{0,1:T(2,128)} %param.22) | copy-start | bytes 4612

commit v3 on v2

v3 whole, which is shorter than its diff:
```python
import functools
import math

import jax
import jax.numpy as jnp
from jax import lax
from jax.experimental import pallas as pl
from jax.experimental.pallas import tpu as pltpu
from jax.sharding import Mesh, PartitionSpec as P

EPS = 1e-06
NZ, NX, NC, NT = 8, 4, 2, 4
EP = ("z", "x", "core")
BLOCK = 256
HALF = BLOCK // 2
CHUNK = NC * BLOCK
COLS = 2 * NX * HALF
ACC = 144
COLS_T = 512
FULL, TAIL = 8, 2
NEAR = (0, 1, 7, 2, 6, 3, 5, 4)
PLUS = (0, 7, 6, 5)
LOW = -1e30
EXP2_SCALE = 64 ** (-0.5) * math.log2(math.e)


def pieces_of(value):
    first = value.astype(jnp.bfloat16).astype(jnp.float32)
    second = (value - first).astype(jnp.bfloat16).astype(jnp.float32)
    third = value - first - second
    return first, second, third


def places():
    return tuple(lax.axis_index(name) for name in (*EP, "tp"))


def remote(source, target, send, receive, device):
    return pltpu.make_async_remote_copy(
        src_ref=source,
        dst_ref=target,
        send_sem=send,
        recv_sem=receive,
        device_id=device,
        device_id_type=pl.DeviceIdType.MESH,
    )


def greet_all(z, x, c, t):
    me = (z * NX + x) * NC + c
    barrier = pltpu.get_barrier_semaphore()

    def signal(step, carry):
        peer = lax.rem(me + step, NZ * NX * NC)
        device = (peer // (NX * NC), lax.rem(peer // NC, NX), lax.rem(peer, NC), t)
        pl.semaphore_signal(
            barrier, inc=1, device_id=device, device_id_type=pl.DeviceIdType.MESH
        )
        return carry

    for dy in (1, NT - 1):
        pl.semaphore_signal(
            barrier,
            inc=1,
            device_id=(z, x, c, lax.rem(t + dy, NT)),
            device_id_type=pl.DeviceIdType.MESH,
        )
    lax.fori_loop(1, NZ * NX * NC, signal, 0)
    pl.semaphore_wait(barrier, NZ * NX * NC + 1)


def columns_of(t):
    return pl.ds(pl.multiple_of(t * COLS_T, COLS_T), COLS_T)


def dispatch_kernel(
    main_ref, tail_ref, pair_ref, query_ref, gate_ref, up_ref, down_ref,
    fmain, ftail, pairs, parts, xmain, xtail, taken, hidden, gate, up, down,
    w_sem, own_sem, out_send, out_recv, y_send, y_recv, kv_send, kv_recv, c_send, c_recv, q_send, q_recv,
):
    z, x, c, t = places()
    me = (z * NX + x) * NC + c
    local = x * NC + c
    group = NX * NC
    after, before = lax.rem(t + 1, NT), lax.rem(t + NT - 1, NT)
    own = columns_of(t)
    own_copies = [
        pltpu.make_async_copy(main_ref.at[me], xmain.at[me, :, own], own_sem.at[0]),
        pltpu.make_async_copy(tail_ref.at[me], xtail.at[me, :, own], own_sem.at[1]),
        pltpu.make_async_copy(pair_ref, pairs.at[z * NC + c], own_sem.at[2]),
        pltpu.make_async_copy(query_ref.at[0], parts.at[0, 0], own_sem.at[3]),
    ]
    weight_copies = [
        pltpu.make_async_copy(source, target, w_sem.at[k])
        for k, (source, target) in enumerate(((gate_ref, gate), (up_ref, up), (down_ref, down)))
    ]
    for copy in own_copies + weight_copies:
        copy.start()
    greet_all(z, x, c, t)

    for dz in (1, 7, 2, 6, 3, 5, 4, 0):
        to_z = lax.rem(z + dz, NZ)

        def send(step, carry):
            peer = lax.rem(local + step, group)
            device = (to_z, peer // NC, lax.rem(peer, NC), t)
            slab = to_z * group + peer
            for k, (source, target) in enumerate(((main_ref, xmain), (tail_ref, xtail))):
                remote(
                    source.at[slab], target.at[me, :, own],
                    out_send.at[k], out_recv.at[k, dz], device,
                ).start()
            return carry

        lax.fori_loop(1 if dz == 0 else 0, group, send, 0)

    mirrored = (NZ - 1 - z, x, c, t)
    remote(query_ref.at[1], parts.at[1, 0], q_send.at[3], q_recv.at[3], mirrored).start()
    for k in range(1, NX):
        device = (z, lax.rem(x + k, NX), c, t)
        remote(query_ref.at[0], parts.at[0, k], q_send.at[k - 1], q_recv.at[k - 1], device).start()

    higher, lower = (lax.rem(z + 1, NZ), x, c, t), (lax.rem(z + NZ - 1, NZ), x, c, t)
    across = (z, x, 1 - c, t)
    for way, device in enumerate((higher, lower)):
        remote(
            pair_ref, pairs.at[z * NC + c], kv_send.at[way, 0], kv_recv.at[way, 0], device
        ).start()
    remote(pair_ref, pairs.at[z * NC + c], c_send.at[0], c_recv.at[0], across).start()

    def rows_of(dz):
        return pl.ds(lax.rem(z - dz + NZ, NZ) * group, group)

    def y_copies(dz, slot, columns, device):
        rows = rows_of(dz)
        return [
            remote(
                target.at[rows, :, columns], target.at[rows, :, columns],
                y_send.at[slot, dz, k], y_recv.at[slot, dz, k], device,
            )
            for k, target in enumerate((xmain, xtail))
        ]

    to_after, to_before = (z, x, c, after), (z, x, c, before)

    def y_relay(dz):
        first = y_copies(dz, 0 if dz in PLUS else 1, own, to_after)
        for copy in first:
            copy.wait_recv()
        if dz in PLUS:
            copies = y_copies(dz, 2, columns_of(before), to_after)
        else:
            copies = y_copies(dz, 2, columns_of(after), to_before)
        for copy in copies:
            copy.start()

    def kv_step(step):
        for way, device in enumerate((higher, lower)):
            back = NZ - step if way == 0 else step
            block = lax.rem(z + back, NZ) * NC + c
            if step < 4:
                here = pairs.at[block]
                onward = here
                if step == 3:
                    onward = pairs.at[block, pl.ds(way * BLOCK, BLOCK), :]
            else:
                here = pairs.at[block, pl.ds(way * BLOCK, BLOCK), :]
            remote(
                here, here, kv_send.at[way, step - 1], kv_recv.at[way, step - 1], device
            ).wait_recv()
            if step < 4:
                remote(
                    onward, onward, kv_send.at[way, step], kv_recv.at[way, step], device
                ).start()
            slot = 2 * step - 1 + way
            remote(here, here, c_send.at[slot], c_recv.at[slot], across).start()

    for copy in own_copies:
        copy.wait()
    for index, dz in enumerate(NEAR):
        count = group - 1 if dz == 0 else group
        first = 0 if dz == 0 else lax.rem(z - dz + NZ, NZ) * group
        rows = pl.ds(first, count)
        for k, (source, target) in enumerate(((main_ref, xmain), (tail_ref, xtail))):
            remote(
                source.at[pl.ds(0, count)], target.at[rows, :, own],
                out_send.at[k], out_recv.at[k, dz], higher,
            ).wait_recv()
        for slot, device in enumerate((to_after, to_before)):
            for copy in y_copies(dz, slot, own, device):
                copy.start()
        if index == 1:
            remote(
                query_ref.at[1], parts.at[1, 0], q_send.at[3], q_recv.at[3], mirrored
            ).wait_recv()
            for k in range(1, NX):
                device = (z, lax.rem(x + k, NX), c, t)
                remote(
                    parts.at[1, 0], parts.at[1, k], q_send.at[3 + k], q_recv.at[3 + k], device
                ).start()
        if index >= 2:
            y_relay(NEAR[index - 2])
    kv_step(1)
    y_relay(NEAR[6])
    y_relay(NEAR[7])
    kv_step(2)
    for dz in NEAR:
        for copy in y_copies(dz, 1 if dz in PLUS else 0, own, to_after):
            copy.wait_recv()
        for copy in y_copies(dz, 2, own, to_after):
            copy.wait_recv()
    for copy in weight_copies:
        copy.wait()
    slabs, width = NZ * group, hidden.shape[1]
    taken[0 : slabs * FULL] = xmain[...].reshape(slabs * FULL, NT * COLS_T)
    taken[slabs * FULL :] = xtail[...].reshape(slabs * TAIL, NT * COLS_T)
    for first in range(0, width, 256):
        cols = slice(first, min(first + 256, width))
        gate_act = jnp.dot(taken[...], gate[:, cols], preferred_element_type=jnp.float32)
        up_act = jnp.dot(taken[...], up[:, cols], preferred_element_type=jnp.float32)
        value = gate_act / (1.0 + jnp.exp(-gate_act)) * up_act
        hidden[:, cols] = value.astype(jnp.bfloat16)
        if first == 256:
            kv_step(3)
    for first in range(0, NT * COLS_T, 256):
        cols = slice(first, first + 256)
        out = jnp.dot(hidden[...], down[:, cols], preferred_element_type=jnp.float32)
        out = out.astype(jnp.bfloat16)
        fmain[:, :, cols] = out[: slabs * FULL].reshape(slabs, FULL, 256)
        ftail[:, :, cols] = out[slabs * FULL :].reshape(slabs, TAIL, 256)
    kv_step(4)

    for dz in NEAR:
        for slot in range(3):
            for copy in y_copies(dz, slot, own, to_after):
                copy.wait_send()
    for k, (source, target) in enumerate(((main_ref, xmain), (tail_ref, xtail))):
        every = pl.ds(0, NZ * group - 1)
        remote(
            source.at[every], target.at[every, :, own], out_send.at[k], out_recv.at[k, 0], higher
        ).wait_send()
    for way in range(2):
        for step in range(4):
            block = pairs.at[0] if step < 3 else pairs.at[0, pl.ds(0, BLOCK), :]
            remote(block, block, kv_send.at[way, step], kv_recv.at[way, step], higher).wait_send()
    for slot in range(9):
        block = pairs.at[0] if slot < 7 else pairs.at[0, pl.ds(0, BLOCK), :]
        copy = remote(block, block, c_send.at[slot], c_recv.at[slot], across)
        copy.wait_send()
        copy.wait_recv()
    for slot in range(7):
        copy = remote(parts.at[0, 0], parts.at[0, 0], q_send.at[slot], q_recv.at[slot], higher)
        copy.wait_send()
        if slot != 3:
            copy.wait_recv()


VMEM = pl.BlockSpec(memory_space=pltpu.VMEM)
HBM = pl.BlockSpec(memory_space=pl.ANY)


def dispatch_call(main, tail, pair, queries, gate, up, down):
    dma = pltpu.SemaphoreType.DMA
    slabs, width = NZ * NX * NC, NT * COLS_T
    units = gate.shape[1]
    return pl.pallas_call(
        dispatch_kernel,
        out_shape=(
            jax.ShapeDtypeStruct((slabs, FULL, width), jnp.bfloat16),
            jax.ShapeDtypeStruct((slabs, TAIL, width), jnp.bfloat16),
            jax.ShapeDtypeStruct((NZ * NC, 2 * BLOCK, BLOCK), jnp.bfloat16),
            jax.ShapeDtypeStruct((2, NX, BLOCK, HALF), jnp.bfloat16),
        ),
        in_specs=[VMEM] * 4 + [HBM] * 3,
        out_specs=(VMEM,) * 4,
        scratch_shapes=[
            pltpu.VMEM((slabs, FULL, width), jnp.bfloat16),
            pltpu.VMEM((slabs, TAIL, width), jnp.bfloat16),
            pltpu.VMEM((slabs * (FULL + TAIL), width), jnp.bfloat16),
            pltpu.VMEM((slabs * (FULL + TAIL), units), jnp.bfloat16),
            pltpu.VMEM((width, units), jnp.bfloat16),
            pltpu.VMEM((width, units), jnp.bfloat16),
            pltpu.VMEM((units, width), jnp.bfloat16),
            dma((3,)), dma((4,)), dma((2,)), dma((2, NZ)), dma((3, NZ, 2)), dma((3, NZ, 2)),
            dma((2, 4)), dma((2, 4)), dma((9,)), dma((9,)), dma((7,)), dma((7,)),
        ],
        compiler_params=pltpu.CompilerParams(
            collective_id=0, has_side_effects=True, vmem_limit_bytes=44 * 2**20
        ),
        name="dispatch",
    )(main, tail, pair, queries, gate, up, down)


def main_kernel(
    lambda_ref, gain_ref, fmain, ftail, query_ref, pair_ref, weight_ref,
    out_ref, rmain, rtail,
    rhs_ref, max_ref, acc_ref, partial, parts,
    attended, upper_send, upper_recv, blocks, relayed, totals, arrived_y,
    relay_main, relay_tail, sum_main, sum_tail, in_main, in_tail, red_main, red_tail,
    own_sem, p_send, p_recv, relay_send, relay_recv, y_send, y_recv, out_send, out_recv,
    u_send, u_recv, mix_send, mix_recv, sum_send, sum_recv,
):
    z, x, c, t = places()
    me = (z * NX + x) * NC + c
    local = x * NC + c
    group = NX * NC
    after, before = lax.rem(t + 1, NT), lax.rem(t + NT - 1, NT)
    opposite = lax.rem(t + 2, NT)
    to_after, to_before = (z, x, c, after), (z, x, c, before)
    devices = (to_after, to_before)
    mirrored = (NZ - 1 - z, x, c, t)
    greet_all(z, x, c, t)
    far = NEAR[::-1]
    pairs = (
        (fmain, relay_main, sum_main, in_main, red_main, rmain),
        (ftail, relay_tail, sum_tail, in_tail, red_tail, rtail),
    )

    def rows_of(dz):
        return pl.ds(lax.rem(z + dz, NZ) * group, group)

    def relay_copy(dz, k):
        source, target = pairs[k][0], pairs[k][1]
        return remote(
            source.at[rows_of(dz), :, columns_of(opposite)], target.at[dz],
            relay_send.at[dz, k], relay_recv.at[dz, k],
            to_after if dz in PLUS else to_before,
        )

    def y_copy(dz, k, way, source):
        return remote(
            source, pairs[k][3].at[way, dz], y_send.at[way, dz, k], y_recv.at[way, dz, k],
            (to_after, to_before)[way],
        )

    def direct(dz, k):
        way = 1 if dz in PLUS else 0
        columns = columns_of((after, before)[way])
        return y_copy(dz, k, way, pairs[k][0].at[rows_of(dz), :, columns])

    for dz in far:
        for k in range(2):
            relay_copy(dz, k).start()
    for dz in far:
        for k in range(2):
            direct(dz, k).start()

    def add_relay(dz):
        way = 0 if dz in PLUS else 1
        columns = columns_of((after, before)[way])
        for k in range(2):
            relay_copy(dz, k).wait_recv()
            source, relayed, total = pairs[k][:3]
            mine = source[rows_of(dz), :, columns].astype(jnp.float32)
            total[dz] = (mine + relayed[dz].astype(jnp.float32)).astype(jnp.bfloat16)
            y_copy(dz, k, way, total.at[dz]).start()

    def finish(dz):
        to_z = lax.rem(z + dz, NZ)
        for k in range(2):
            source, arrived, reduced = pairs[k][0], pairs[k][3], pairs[k][4]
            for way in range(2):
                y_copy(dz, k, way, pairs[k][2].at[dz]).wait_recv()
            reduced[rows_of(dz)] = (
                source[rows_of(dz), :, columns_of(t)].astype(jnp.float32)
                + arrived[0, dz].astype(jnp.float32)
                + arrived[1, dz].astype(jnp.float32)
            ).astype(jnp.bfloat16)

        def send(step, carry):
            peer = lax.rem(local + step, group)
            device = (to_z, peer // NC, lax.rem(peer, NC), t)
            for k in range(2):
                remote(
                    pairs[k][4].at[to_z * group + peer], pairs[k][5].at[me],
                    out_send.at[k], out_recv.at[k], device,
                ).start()
            return carry

        lax.fori_loop(1 if dz == 0 else 0, group, send, 0)
        if dz == 0:
            for k in range(2):
                pltpu.make_async_copy(
                    pairs[k][4].at[me], pairs[k][5].at[me], own_sem.at[k]
                ).start()

    map_row = lax.broadcasted_iota(jnp.int32, (128, HALF), 0)
    for way in range(2):
        for head in range(2):
            for step in range(NX):
                block = query_ref[way, step, head * 128 : (head + 1) * 128, :]
                for which in range(2):
                    first = (which * NX + step) * HALF
                    keep = (map_row < 64) if which == 0 else (map_row >= 64)
                    rhs_ref[head, way, :, first : first + HALF] = jnp.where(
                        keep, block, jnp.zeros_like(block)
                    )
    max_ref[...] = jnp.full_like(max_ref, LOW)
    acc_ref[...] = jnp.zeros_like(acc_ref)
    ones = jnp.ones((ACC - 128, CHUNK), jnp.bfloat16)
    tile = 256
    units = NZ + 1

    def work(head, way, step_z, masked):
        lanes = pl.ds(pl.multiple_of(head * 128, 128), 128)
        below = pl.ds(pl.multiple_of(256 + head * 128, 128), 128)
        keys = [pair_ref[step_z * NC + k, 0:256, lanes] for k in range(NC)]
        values = [pair_ref[step_z * NC + k, below, :] for k in range(NC)]
        keys = jnp.concatenate(keys, axis=0)
        values = jnp.concatenate([jnp.concatenate(values, axis=1), ones], axis=0)
        for first in range(0, COLS, tile):
            cols = slice(first, first + tile)
            scores = jnp.dot(keys, rhs_ref[head, way, :, cols], preferred_element_type=jnp.float32)
            if masked:
                key = lax.broadcasted_iota(jnp.int32, (CHUNK, tile), 0) + 2 * BLOCK * x
                col = lax.broadcasted_iota(jnp.int32, (1, tile), 1) + first
                query_x = lax.rem(x - (col // HALF) % NX + NX, NX)
                position = (2 * query_x + c) * BLOCK + way * HALF + col % HALF
                scores = jnp.where(position >= key, scores, -3e38)
            earlier = max_ref[way, 0:1, cols]
            now = jnp.maximum(earlier, jnp.max(scores, axis=0, keepdims=True))
            weights = jnp.exp2((scores - now) * EXP2_SCALE).astype(jnp.bfloat16)
            rescale = jnp.exp2((earlier - now) * EXP2_SCALE)
            max_ref[way, 0:1, cols] = now
            acc_ref[way, :, cols] = acc_ref[way, :, cols] * rescale + jnp.dot(
                values, weights, preferred_element_type=jnp.float32
            )

    def x_copy(head, k):
        maps = pl.ds(2 * head, 2)
        device = (z, lax.rem(x + NX - k, NX), c, t)
        return remote(
            partial.at[k, maps], parts.at[k - 1, maps],
            p_send.at[head, k - 1], p_recv.at[head, k - 1], device,
        )

    def send_partial(head):
        row = lax.broadcasted_iota(jnp.int32, (ACC - 128, COLS), 0)
        for way in range(2):
            stats = jnp.zeros((ACC - 128, COLS), jnp.float32)
            pieces = pieces_of(acc_ref[way, 128:129, :]) + pieces_of(max_ref[way, 0:1, :])
            for index, piece in enumerate(pieces):
                stats = jnp.where(row == index, piece, stats)
            for which in range(2):
                for step in range(NX):
                    first = (which * NX + step) * HALF
                    lanes = slice(way * HALF, (way + 1) * HALF)
                    partial[step, 2 * head + which, 0:128, lanes] = acc_ref[
                        way, 0:128, first : first + HALF
                    ].astype(jnp.bfloat16)
                    partial[step, 2 * head + which, 128:ACC, lanes] = stats[
                        :, first : first + HALF
                    ].astype(jnp.bfloat16)
        for k in range(1, NX):
            x_copy(head, k).start()

    def unit(index, carry):
        head = index // units
        step = lax.rem(index, units)
        way = jnp.where(step > z, 1, 0)
        step_z = jnp.where(step > z, step - z - 1, step)
        last = (step == z) | (step == units - 1)

        @pl.when(last)
        def _():
            work(head, way, step_z, True)

        @pl.when(jnp.logical_not(last))
        def _():
            work(head, way, step_z, False)

        for k, dz in enumerate(far):

            @pl.when(index == 2 * k)
            def _():
                add_relay(dz)

            @pl.when(index == 2 * k + 2)
            def _():
                finish(dz)

        @pl.when(index == units - 1)
        def _():
            send_partial(0)
            max_ref[...] = jnp.full_like(max_ref, LOW)
            acc_ref[...] = jnp.zeros_like(acc_ref)

        return carry

    lax.fori_loop(0, 2 * units, unit, 0)
    send_partial(1)

    for head in range(2):
        for k in range(1, NX):
            x_copy(head, k).wait_recv()
        per_map = []
        for which in range(2):
            index = 2 * head + which
            sources = [partial.at[0, index]] + [parts.at[k, index] for k in range(NX - 1)]
            totals_of, maxima = [], []
            for part in sources:
                stats = part[128:ACC, :].astype(jnp.float32)
                totals_of.append(stats[0:1] + stats[1:2] + stats[2:3])
                maxima.append(stats[3:4] + stats[4:5] + stats[5:6])
            largest = functools.reduce(jnp.maximum, maxima)
            total, numerator = 0.0, 0.0
            for part, own_total, own_max in zip(sources, totals_of, maxima):
                factor = jnp.exp2((own_max - largest) * EXP2_SCALE)
                total = total + factor * own_total
                numerator = numerator + factor * part[0:128, :].astype(jnp.float32)
            per_map.append(numerator / total)
        contrast = per_map[0] - lambda_ref[head] * per_map[1]
        square = jnp.mean(contrast * contrast, axis=0, keepdims=True)
        normed = contrast * lax.rsqrt(square + EPS) * gain_ref[...]
        normed = normed.astype(jnp.bfloat16)
        attended[head * 128 : (head + 1) * 128, :] = normed[:, :HALF]
        upper_send[head * 128 : (head + 1) * 128, :] = normed[:, HALF:]

    flip = remote(upper_send, upper_recv, u_send, u_recv, mirrored)
    flip.start()
    rows = BLOCK // NT
    half = rows // 2

    def project(source, first):
        for low in range(0, 2048, 512):
            part = lax.dot_general(
                source[...], weight_ref[:, low : low + 512],
                (((0,), (0,)), ((), ())), preferred_element_type=jnp.float32,
            ).astype(jnp.bfloat16)
            blocks[first, :, low : low + 512] = part[:rows]
            blocks[first + 1, :, low : low + 512] = part[rows:]

    project(attended, 0)
    flip.wait()
    project(upper_recv, 2)

    def mix_relay(way):
        return remote(
            blocks.at[opposite, pl.ds(way * half, half), :], relayed.at[way],
            mix_send.at[way], mix_recv.at[way], devices[way],
        )

    def mix_copy(way, part, source):
        return remote(
            source, arrived_y.at[way, pl.ds(part * half, half), :],
            sum_send.at[way, part], sum_recv.at[way, part], devices[way],
        )

    for way in range(2):
        mix_relay(way).start()
    for way in range(2):
        source = blocks.at[(after, before)[way], pl.ds((1 - way) * half, half), :]
        mix_copy(way, 1 - way, source).start()
    for way in range(2):
        mix_relay(way).wait_recv()
        mine = blocks[(after, before)[way], way * half : (way + 1) * half, :]
        totals[way] = (
            mine.astype(jnp.float32) + relayed[way].astype(jnp.float32)
        ).astype(jnp.bfloat16)
        mix_copy(way, way, totals.at[way]).start()
    for way in range(2):
        for part in range(2):
            copy = mix_copy(way, part, totals.at[way])
            copy.wait_recv()
            copy.wait_send()
        mix_relay(way).wait_send()
    out_ref[...] = (
        blocks[t].astype(jnp.float32)
        + arrived_y[0].astype(jnp.float32)
        + arrived_y[1].astype(jnp.float32)
    ).astype(jnp.bfloat16)

    for k in range(2):
        pltpu.make_async_copy(pairs[k][4].at[me], pairs[k][5].at[me], own_sem.at[k]).wait()
        every = pl.ds(0, NZ * group - 1)
        copy = remote(
            pairs[k][4].at[every], pairs[k][5].at[every], out_send.at[k], out_recv.at[k], to_after
        )
        copy.wait_recv()
        copy.wait_send()
        for dz in far:
            relay_copy(dz, k).wait_send()
            for way in range(2):
                y_copy(dz, k, way, pairs[k][2].at[dz]).wait_send()
    for head in range(2):
        for k in range(1, NX):
            x_copy(head, k).wait_send()


def main_call(head_lambda, sub_gain, fmain, ftail, queries, pairs, out_weight):
    dma = pltpu.SemaphoreType.DMA
    slabs = NZ * NX * NC
    group = NX * NC
    rows, width = BLOCK // NT, out_weight.shape[1]
    bf16, f32 = jnp.bfloat16, jnp.float32

    def both(*lead):
        return [pltpu.VMEM((*lead, count, COLS_T), bf16) for count in (FULL, TAIL)]

    return pl.pallas_call(
        main_kernel,
        out_shape=(
            jax.ShapeDtypeStruct((rows, width), bf16),
            jax.ShapeDtypeStruct((slabs, FULL, COLS_T), bf16),
            jax.ShapeDtypeStruct((slabs, TAIL, COLS_T), bf16),
        ),
        in_specs=[pl.BlockSpec(memory_space=pltpu.SMEM)] + [VMEM] * 6,
        out_specs=(VMEM,) * 3,
        scratch_shapes=[
            pltpu.VMEM((2, 2, 128, COLS), bf16),
            pltpu.VMEM((2, 8, COLS), f32),
            pltpu.VMEM((2, ACC, COLS), f32),
            pltpu.VMEM((NX, 4, ACC, BLOCK), bf16),
            pltpu.VMEM((NX - 1, 4, ACC, BLOCK), bf16),
            pltpu.VMEM((BLOCK, HALF), bf16),
            pltpu.VMEM((BLOCK, HALF), bf16),
            pltpu.VMEM((BLOCK, HALF), bf16),
            pltpu.VMEM((NT, rows, width), bf16),
            pltpu.VMEM((2, rows // 2, width), bf16),
            pltpu.VMEM((2, rows // 2, width), bf16),
            pltpu.VMEM((2, rows, width), bf16),
            *both(NZ, group), *both(NZ, group), *both(2, NZ, group), *both(slabs),
            dma((2,)), dma((2, 3)), dma((2, 3)), dma((NZ, 2)), dma((NZ, 2)),
            dma((2, NZ, 2)), dma((2, NZ, 2)), dma((2,)), dma((2,)),
            dma(()), dma(()), dma((2,)), dma((2,)), dma((2, 2)), dma((2, 2)),
        ],
        compiler_params=pltpu.CompilerParams(
            collective_id=1, has_side_effects=True, vmem_limit_bytes=44 * 2**20
        ),
        name="mixer",
    )(head_lambda, sub_gain[:, None], fmain, ftail, queries, pairs, out_weight)


def shards(
    queries,
    key_rows,
    value_rows,
    head_lambda,
    sub_gain,
    out_weight,
    expert_input,
    norm_gain,
    route_ids,
    route_weight,
    gate_weight,
    up_weight,
    down_weight,
):
    rows_here, model_width = expert_input.shape
    experts = NZ * NX * NC
    top_count = route_ids.shape[1]
    slots = experts * (FULL + TAIL)
    wide_rows = expert_input.astype(jnp.float32)
    normed = (
        wide_rows
        * lax.rsqrt(jnp.mean(wide_rows * wide_rows, axis=-1, keepdims=True) + EPS)
        * norm_gain
    ).astype(jnp.bfloat16)
    flat_ids = route_ids.reshape(-1)
    onehot = (flat_ids[:, None] == jnp.arange(experts, dtype=jnp.int32)[None, :]).astype(jnp.int32)
    rank_before = jnp.cumsum(onehot, axis=0) - onehot
    slot = jnp.sum(rank_before * onehot, axis=1)
    buffer_pos = jnp.where(
        slot < FULL,
        flat_ids * FULL + slot,
        experts * FULL + flat_ids * TAIL + slot - FULL,
    ).reshape(rows_here, top_count)
    matches = buffer_pos[None, :, :] == jnp.arange(slots, dtype=jnp.int32)[:, None, None]
    dispatch = jnp.any(matches, axis=-1).astype(jnp.bfloat16)
    combine = jnp.sum(jnp.where(matches, route_weight[None, :, :], 0.0), axis=-1)
    own_cols = lax.dynamic_slice_in_dim(normed, lax.axis_index("tp") * COLS_T, COLS_T, 1)
    outgoing = jnp.dot(dispatch, own_cols, preferred_element_type=jnp.float32).astype(jnp.bfloat16)
    main = outgoing[: experts * FULL].reshape(experts, FULL, COLS_T)
    tail = outgoing[experts * FULL :].reshape(experts, TAIL, COLS_T)
    pair = jnp.concatenate([key_rows, value_rows.T], axis=0)
    turned = queries.T
    halves = jnp.stack([turned[:, :HALF], turned[:, HALF:]])

    fmain, ftail, pairs, parts = dispatch_call(
        main, tail, pair, halves, gate_weight[0], up_weight[0], down_weight[0]
    )
    mixer_out, rmain, rtail = main_call(
        head_lambda, sub_gain, fmain, ftail, parts, pairs, out_weight
    )
    returned = jnp.concatenate(
        [rmain.reshape(experts * FULL, COLS_T), rtail.reshape(experts * TAIL, COLS_T)], axis=0
    )
    mixed = lax.dot_general(
        combine,
        returned.astype(jnp.float32),
        (((0,), (0,)), ((), ())),
        preferred_element_type=jnp.float32,
    )
    return (mixer_out, mixed.astype(jnp.bfloat16))


def solution(mesh):
    mesh = Mesh(mesh.devices.reshape(NZ, NX, NC, NT), (*EP, "tp"))
    placed = (
        P(EP, "tp"),
        P(EP, "tp"),
        P(EP, "tp"),
        P("tp"),
        P(),
        P("tp", None),
        P(EP, None),
        P(),
        P(EP, None),
        P(EP, None),
        P(EP, None, "tp"),
        P(EP, None, "tp"),
        P(EP, "tp", None),
    )
    return jax.shard_map(
        shards,
        mesh=mesh,
        in_specs=placed,
        out_specs=(P((*EP, "tp"), None), P(EP, "tp")),
        check_vma=False,
    )
```

time: 190 us -> 165 us (0.87)
  Pallas kernels: 162 us -> 145 us
  local copies, waits for them, and re-layouts: 19.6 us -> 12.2 us
    pallas_call x4 -> x1, Pallas kernels: 99 us -> 80.1 us  [main_call(): pl.pallas_call(main_kernel, out_shape=(jax.ShapeDtypeStruct((rows, width)...]
    unnamed x36 -> x30, local copies, waits for them, and re-layouts: 13.9 us -> 10.3 us
    reshape x2 -> x0, local copies, waits for them, and re-layouts: 3.18 us -> none  [the longest x1 2.19 us: shards(): ftail.reshape(experts, TAIL, model_width)]
    pallas_call x1, Pallas kernels: 62.7 us -> 64.7 us  [dispatch_call(): pl.pallas_call(dispatch_kernel, out_shape=(jax.ShapeDtypeStruct((slabs, F...]
where the time goes in v3:
time: 165 us; the launch traced here: 163 us
  Pallas kernels  145 us (88%)
  local copies, waits for them, and re-layouts  12.2 us (7%)
  other arithmetic  2.55 us (2%)
  matrix products  2.49 us (2%)
    pallas_call x1, Pallas kernels, main_call(): pl.pallas_call(main_kernel, out_shape=(jax.ShapeDtypeStruct((rows, width)...  80.1 us
    pallas_call x1, Pallas kernels, dispatch_call(): pl.pallas_call(dispatch_kernel, out_shape=(jax.ShapeDtypeStruct((slabs, F...  64.7 us
    unnamed x30, local copies, waits for them, and re-layouts  10.3 us

profile of v3, /device:TPU:2, one launch (start us, length us, event | category | flops | bytes accessed | tf_op | source)
XLA Modules:
  0.0 162.9 jit_solution(14196068210336986713)
XLA Ops:
  0.6 0.0 copy-start.7
  0.6 0.8 dynamic-slice
  1.5 0.8 copy.44
  2.3 0.1 eq.42
  2.4 0.9 reduce-window.6
  3.3 0.2 slice_reduce_fusion
  3.6 0.1 eq.38
  3.8 0.1 fusion.11
  3.9 0.1 reduce_sum.30
  4.0 0.1 copy.47
  4.1 0.7 compare_select_fusion
  4.8 0.1 fusion
  5.0 0.0 copy-done.7
  5.0 0.2 convert_element_type.23
  5.1 0.0 copy-start.8
  5.2 0.2 multiply_reduce_fusion
  5.4 0.0 copy-start.9
  5.4 0.4 convolution_convert_fusion
  5.9 0.0 copy-start.10
  5.9 0.1 reshape.60.tail_ref
  6.0 0.1 copy-done.8
  6.0 0.1 copy.51
  6.2 0.1 copy-done.9
  6.3 0.1 copy.50
  6.4 0.4 copy-done.10
  6.8 0.0 copy-start.1
  6.8 2.0 %copy-done.1 = bf16[1,2048,896]{2,1,0:T(8,128)(2,1)S(1)} copy-done((bf16[1,2048,896]{2,1,0:T(8,128)(2,1)S(1)}, bf16[1,2048,896]{2,1,0:T(8,128)(2,1)}, u32[]{:S(2)}) %copy-start.1) | copy-done | bytes 3670040
  8.9 0.0 copy-start.12
  8.9 0.0 copy-start.5
  8.9 64.7 %dispatch.1 = (bf16[64,8,2048]{2,1,0:T(8,128)(2,1)S(1)}, bf16[64,2,2048]{2,1,0:T(2,128)(2,1)S(1)}, bf16[16,512,256]{2,1,0:T(8,128)(2,1)}, bf16[2,4,256,128]{3,2,1,0:T(8,128)(2,1)S(1)}) custom-call(bf16[64,8,512]{2,1,0:T(8,128)(2,1)S(1)} %slice_bitcast_fusion.main_ref, bf16[64,2,512]{2,1,0:T(2,128)(2,1)S(1)} %reshape.60.tail_ref, ...), custom_call_target="tpu_custom_call" | custom-call | tf_op jit(solution)/shard_map/dispatch/pallas_call | solution.py:266
  73.6 0.0 copy-start.3
  73.6 0.8 copy-done.3
  74.4 0.0 copy-done.12
  74.4 0.1 copy.52.gain_ref
  74.5 0.0 copy-done.5
  74.5 0.0 copy-start
  74.5 2.2 %copy-done = bf16[16,512,256]{2,1,0:T(8,128)(2,1)S(1)} copy-done((bf16[16,512,256]{2,1,0:T(8,128)(2,1)S(1)}, bf16[16,512,256]{2,1,0:T(8,128)(2,1)}, u32[]{:S(2)}) %copy-start) | copy-done | bytes 4194328
  76.7 0.0 copy-start.2
  76.7 1.2 copy-done.2
  77.9 0.0 copy-start.4
  77.9 1.0 copy-done.4
  79.0 0.0 copy-start.11
  79.0 80.1 %mixer.1 = (bf16[64,2048]{1,0:T(8,128)(2,1)S(1)}, bf16[64,8,512]{2,1,0:T(8,128)(2,1)S(1)}, bf16[64,2,512]{2,1,0:T(2,128)(2,1)S(1)}) custom-call(f32[2]{0:T(128)S(1)} %copy-done.5, f32[128,1]{1,0:T(8,128)S(1)} %copy.52.gain_ref, bf16[64,8,2048]{2,1,0:T(8,128)(2,1)S(1)} %get-tuple-element.9.fmain, bf16[64,2,2048]{2,1,0:T(2,128)(2,1)S(1)} %get-tuple-element.10.ftail, ...), custom_call_target="tpu_custom_call" | custom-call | tf_op jit(solution)/shard_map/mixer/pallas_call | solution.py:600
  159.1 0.0 copy-start.6
  159.1 0.8 copy-done.6
  159.9 0.1 reshape.62
  159.9 0.0 copy-done.11
  159.9 0.2 select_reduce_fusion
  160.1 2.0 %convolution_convert_fusion.1 = bf16[192,512]{1,0:T(8,128)(2,1)} fusion(bf16[640,192]{0,1:T(8,128)(2,1)S(1)} %select_reduce_fusion, bf16[128,512]{1,0:T(8,128)(2,1)S(1)} %reshape.62, bf16[512,512]{1,0:T(8,128)(2,1)} %bitcast.36), kind=kOutput, calls=%fused_computation.2 | convolution fusion | flops 127139840 | bytes 1097728 | tf_op jit(solution)/shard_map/dot_general | solution.py:688
  162.2 0.7 copy.56
  (8 shorter events, 0.2 us)
Async XLA Ops:
  0.6 4.3 %copy-start.7 = (bf16[192,2048]{1,0:T(8,128)(2,1)S(1)}, bf16[192,2048]{1,0:T(8,128)(2,1)}, u32[]{:S(2)}) copy-start(bf16[192,2048]{1,0:T(8,128)(2,1)} %param.19) | copy-start | bytes 2359300
  5.1 0.9 copy-start.8
  5.4 0.9 copy-start.9
  5.9 0.9 copy-start.10
  6.8 2.0 %copy-start.1 = (bf16[1,2048,896]{2,1,0:T(8,128)(2,1)S(1)}, bf16[1,2048,896]{2,1,0:T(8,128)(2,1)}, u32[]{:S(2)}) copy-start(bf16[1,2048,896]{2,1,0:T(8,128)(2,1)} %param.23) | copy-start | bytes 11010052
  8.9 65.6 %copy-start.12 = (f32[128]{0:T(128)S(1)}, f32[128]{0:T(128)}, u32[]{:S(2)}) copy-start(f32[128]{0:T(128)} %param.17) | copy-start | bytes 1540
  8.9 65.7 %copy-start.5 = (f32[2]{0:T(128)S(1)}, f32[2]{0:T(128)}, u32[]{:S(2)}) copy-start(f32[2]{0:T(128)} %lambda_ref.1) | copy-start | bytes 28
  73.6 0.8 copy-start.3
  74.5 2.2 %copy-start = (bf16[16,512,256]{2,1,0:T(8,128)(2,1)S(1)}, bf16[16,512,256]{2,1,0:T(8,128)(2,1)}, u32[]{:S(2)}) copy-start(bf16[16,512,256]{2,1,0:T(8,128)(2,1)} %get-tuple-element.12.pair_ref) | copy-start | bytes 12582916
  76.7 1.2 copy-start.2
  77.9 1.0 copy-start.4
  79.0 80.9 %copy-start.11 = (f32[192,2]{0,1:T(2,128)S(1)}, f32[192,2]{0,1:T(2,128)}, u32[]{:S(2)}) copy-start(f32[192,2]{0,1:T(2,128)} %param.22) | copy-start | bytes 4612
  159.1 0.8 copy-start.6

commit v4 on v3

--- a/solution.py
+++ b/solution.py
@@ -73,10 +73,17 @@
     return pl.ds(pl.multiple_of(t * COLS_T, COLS_T), COLS_T)
 
 
-def dispatch_kernel(
-    main_ref, tail_ref, pair_ref, query_ref, gate_ref, up_ref, down_ref,
-    fmain, ftail, pairs, parts, xmain, xtail, taken, hidden, gate, up, down,
-    w_sem, own_sem, out_send, out_recv, y_send, y_recv, kv_send, kv_recv, c_send, c_recv, q_send, q_recv,
+def layer_kernel(
+    lambda_ref, gain_ref, main_ref, tail_ref, pair_ref, query_ref, weight_ref,
+    gate_ref, up_ref, down_ref,
+    out_ref, rmain, rtail,
+    xmain, xtail, taken, hidden, gate, up, down, fmain, ftail, pairs, parts,
+    rhs_ref, score_ref, max_ref, acc_ref, partial, others,
+    attended, upper_send, upper_recv, blocks, relayed, totals, arrived_y,
+    relay_main, relay_tail, sum_main, sum_tail, in_main, in_tail, red_main, red_tail,
+    w_sem, own_sem, out_send, out_recv, y_send, y_recv, kv_send, kv_recv, c_send, c_recv,
+    q_send, q_recv, r_sem, p_send, p_recv, relay_send, relay_recv, s_send, s_recv,
+    back_send, back_recv, u_send, u_recv, mix_send, mix_recv, sum_send, sum_recv,
 ):
     z, x, c, t = places()
     me = (z * NX + x) * NC + c
@@ -174,6 +181,36 @@
                 ).start()
             slot = 2 * step - 1 + way
             remote(here, here, c_send.at[slot], c_recv.at[slot], across).start()
+
+    opposite = lax.rem(t + 2, NT)
+    devices = (to_after, to_before)
+    far = NEAR[::-1]
+    stages = (
+        (fmain, relay_main, sum_main, in_main, red_main, rmain),
+        (ftail, relay_tail, sum_tail, in_tail, red_tail, rtail),
+    )
+
+    def back_rows(dz):
+        return pl.ds(lax.rem(z + dz, NZ) * group, group)
+
+    def relay_copy(dz, k):
+        source, target = stages[k][0], stages[k][1]
+        return remote(
+            source.at[back_rows(dz), :, columns_of(opposite)], target.at[dz],
+            relay_send.at[dz, k], relay_recv.at[dz, k],
+            to_after if dz in PLUS else to_before,
+        )
+
+    def s_copy(dz, k, way, source):
+        return remote(
+            source, stages[k][3].at[way, dz], s_send.at[way, dz, k], s_recv.at[way, dz, k],
+            (to_after, to_before)[way],
+        )
+
+    def direct(dz, k):
+        way = 1 if dz in PLUS else 0
+        columns = columns_of((after, before)[way])
+        return s_copy(dz, k, way, stages[k][0].at[back_rows(dz), :, columns])
 
     for copy in own_copies:
         copy.wait()
@@ -220,149 +257,39 @@
         up_act = jnp.dot(taken[...], up[:, cols], preferred_element_type=jnp.float32)
         value = gate_act / (1.0 + jnp.exp(-gate_act)) * up_act
         hidden[:, cols] = value.astype(jnp.bfloat16)
-        if first == 256:
-            kv_step(3)
-    for first in range(0, NT * COLS_T, 256):
-        cols = slice(first, first + 256)
-        out = jnp.dot(hidden[...], down[:, cols], preferred_element_type=jnp.float32)
-        out = out.astype(jnp.bfloat16)
-        fmain[:, :, cols] = out[: slabs * FULL].reshape(slabs, FULL, 256)
-        ftail[:, :, cols] = out[slabs * FULL :].reshape(slabs, TAIL, 256)
-    kv_step(4)
-
-    for dz in NEAR:
-        for slot in range(3):
-            for copy in y_copies(dz, slot, own, to_after):
-                copy.wait_send()
-    for k, (source, target) in enumerate(((main_ref, xmain), (tail_ref, xtail))):
-        every = pl.ds(0, NZ * group - 1)
-        remote(
-            source.at[every], target.at[every, :, own], out_send.at[k], out_recv.at[k, 0], higher
-        ).wait_send()
-    for way in range(2):
-        for step in range(4):
-            block = pairs.at[0] if step < 3 else pairs.at[0, pl.ds(0, BLOCK), :]
-            remote(block, block, kv_send.at[way, step], kv_recv.at[way, step], higher).wait_send()
-    for slot in range(9):
-        block = pairs.at[0] if slot < 7 else pairs.at[0, pl.ds(0, BLOCK), :]
-        copy = remote(block, block, c_send.at[slot], c_recv.at[slot], across)
-        copy.wait_send()
-        copy.wait_recv()
-    for slot in range(7):
-        copy = remote(parts.at[0, 0], parts.at[0, 0], q_send.at[slot], q_recv.at[slot], higher)
-        copy.wait_send()
-        if slot != 3:
-            copy.wait_recv()
-
-
-VMEM = pl.BlockSpec(memory_space=pltpu.VMEM)
-HBM = pl.BlockSpec(memory_space=pl.ANY)
-
-
-def dispatch_call(main, tail, pair, queries, gate, up, down):
-    dma = pltpu.SemaphoreType.DMA
-    slabs, width = NZ * NX * NC, NT * COLS_T
-    units = gate.shape[1]
-    return pl.pallas_call(
-        dispatch_kernel,
-        out_shape=(
-            jax.ShapeDtypeStruct((slabs, FULL, width), jnp.bfloat16),
-            jax.ShapeDtypeStruct((slabs, TAIL, width), jnp.bfloat16),
-            jax.ShapeDtypeStruct((NZ * NC, 2 * BLOCK, BLOCK), jnp.bfloat16),
-            jax.ShapeDtypeStruct((2, NX, BLOCK, HALF), jnp.bfloat16),
-        ),
-        in_specs=[VMEM] * 4 + [HBM] * 3,
-        out_specs=(VMEM,) * 4,
-        scratch_shapes=[
-            pltpu.VMEM((slabs, FULL, width), jnp.bfloat16),
-            pltpu.VMEM((slabs, TAIL, width), jnp.bfloat16),
-            pltpu.VMEM((slabs * (FULL + TAIL), width), jnp.bfloat16),
-            pltpu.VMEM((slabs * (FULL + TAIL), units), jnp.bfloat16),
-            pltpu.VMEM((width, units), jnp.bfloat16),
-            pltpu.VMEM((width, units), jnp.bfloat16),
-            pltpu.VMEM((units, width), jnp.bfloat16),
-            dma((3,)), dma((4,)), dma((2,)), dma((2, NZ)), dma((3, NZ, 2)), dma((3, NZ, 2)),
-            dma((2, 4)), dma((2, 4)), dma((9,)), dma((9,)), dma((7,)), dma((7,)),
-        ],
-        compiler_params=pltpu.CompilerParams(
-            collective_id=0, has_side_effects=True, vmem_limit_bytes=44 * 2**20
-        ),
-        name="dispatch",
-    )(main, tail, pair, queries, gate, up, down)
-
-
-def main_kernel(
-    lambda_ref, gain_ref, fmain, ftail, query_ref, pair_ref, weight_ref,
-    out_ref, rmain, rtail,
-    rhs_ref, max_ref, acc_ref, partial, parts,
-    attended, upper_send, upper_recv, blocks, relayed, totals, arrived_y,
-    relay_main, relay_tail, sum_main, sum_tail, in_main, in_tail, red_main, red_tail,
-    own_sem, p_send, p_recv, relay_send, relay_recv, y_send, y_recv, out_send, out_recv,
-    u_send, u_recv, mix_send, mix_recv, sum_send, sum_recv,
-):
-    z, x, c, t = places()
-    me = (z * NX + x) * NC + c
-    local = x * NC + c
-    group = NX * NC
-    after, before = lax.rem(t + 1, NT), lax.rem(t + NT - 1, NT)
-    opposite = lax.rem(t + 2, NT)
-    to_after, to_before = (z, x, c, after), (z, x, c, before)
-    devices = (to_after, to_before)
-    mirrored = (NZ - 1 - z, x, c, t)
-    greet_all(z, x, c, t)
-    far = NEAR[::-1]
-    pairs = (
-        (fmain, relay_main, sum_main, in_main, red_main, rmain),
-        (ftail, relay_tail, sum_tail, in_tail, red_tail, rtail),
-    )
-
-    def rows_of(dz):
-        return pl.ds(lax.rem(z + dz, NZ) * group, group)
-
-    def relay_copy(dz, k):
-        source, target = pairs[k][0], pairs[k][1]
-        return remote(
-            source.at[rows_of(dz), :, columns_of(opposite)], target.at[dz],
-            relay_send.at[dz, k], relay_recv.at[dz, k],
-            to_after if dz in PLUS else to_before,
-        )
-
-    def y_copy(dz, k, way, source):
-        return remote(
-            source, pairs[k][3].at[way, dz], y_send.at[way, dz, k], y_recv.at[way, dz, k],
-            (to_after, to_before)[way],
-        )
-
-    def direct(dz, k):
-        way = 1 if dz in PLUS else 0
-        columns = columns_of((after, before)[way])
-        return y_copy(dz, k, way, pairs[k][0].at[rows_of(dz), :, columns])
-
-    for dz in far:
-        for k in range(2):
-            relay_copy(dz, k).start()
-    for dz in far:
-        for k in range(2):
-            direct(dz, k).start()
-
+    for turn in (2, 1, 3, 0):
+        for part in range(2):
+            start = lax.rem(t + turn, NT) * COLS_T + part * 256
+            cols = pl.ds(pl.multiple_of(start, 256), 256)
+            out = jnp.dot(hidden[...], down[:, cols], preferred_element_type=jnp.float32)
+            out = out.astype(jnp.bfloat16)
+            fmain[:, :, cols] = out[: slabs * FULL].reshape(slabs, FULL, 256)
+            ftail[:, :, cols] = out[slabs * FULL :].reshape(slabs, TAIL, 256)
+        for dz in far:
+            for k in range(2):
+                if turn == 2:
+                    relay_copy(dz, k).start()
+                elif turn == (3 if dz in PLUS else 1):
+                    direct(dz, k).start()
+    kv_step(3)
     def add_relay(dz):
         way = 0 if dz in PLUS else 1
         columns = columns_of((after, before)[way])
         for k in range(2):
             relay_copy(dz, k).wait_recv()
-            source, relayed, total = pairs[k][:3]
-            mine = source[rows_of(dz), :, columns].astype(jnp.float32)
+            source, relayed, total = stages[k][:3]
+            mine = source[back_rows(dz), :, columns].astype(jnp.float32)
             total[dz] = (mine + relayed[dz].astype(jnp.float32)).astype(jnp.bfloat16)
-            y_copy(dz, k, way, total.at[dz]).start()
+            s_copy(dz, k, way, total.at[dz]).start()
 
     def finish(dz):
         to_z = lax.rem(z + dz, NZ)
         for k in range(2):
-            source, arrived, reduced = pairs[k][0], pairs[k][3], pairs[k][4]
+            source, arrived, reduced = stages[k][0], stages[k][3], stages[k][4]
             for way in range(2):
-                y_copy(dz, k, way, pairs[k][2].at[dz]).wait_recv()
-            reduced[rows_of(dz)] = (
-                source[rows_of(dz), :, columns_of(t)].astype(jnp.float32)
+                s_copy(dz, k, way, stages[k][2].at[dz]).wait_recv()
+            reduced[back_rows(dz)] = (
+                source[back_rows(dz), :, columns_of(t)].astype(jnp.float32)
                 + arrived[0, dz].astype(jnp.float32)
                 + arrived[1, dz].astype(jnp.float32)
             ).astype(jnp.bfloat16)
@@ -372,8 +299,8 @@
             device = (to_z, peer // NC, lax.rem(peer, NC), t)
             for k in range(2):
                 remote(
-                    pairs[k][4].at[to_z * group + peer], pairs[k][5].at[me],
-                    out_send.at[k], out_recv.at[k], device,
+                    stages[k][4].at[to_z * group + peer], stages[k][5].at[me],
+                    back_send.at[k], back_recv.at[k], device,
                 ).start()
             return carry
 
@@ -381,14 +308,19 @@
         if dz == 0:
             for k in range(2):
                 pltpu.make_async_copy(
-                    pairs[k][4].at[me], pairs[k][5].at[me], own_sem.at[k]
+                    stages[k][4].at[me], stages[k][5].at[me], r_sem.at[k]
                 ).start()
 
+    for slot in range(7):
+        if slot != 3:
+            remote(
+                parts.at[0, 0], parts.at[0, 0], q_send.at[slot], q_recv.at[slot], higher
+            ).wait_recv()
     map_row = lax.broadcasted_iota(jnp.int32, (128, HALF), 0)
     for way in range(2):
         for head in range(2):
             for step in range(NX):
-                block = query_ref[way, step, head * 128 : (head + 1) * 128, :]
+                block = parts[way, step, head * 128 : (head + 1) * 128, :]
                 for which in range(2):
                     first = (which * NX + step) * HALF
                     keep = (map_row < 64) if which == 0 else (map_row >= 64)
@@ -399,16 +331,17 @@
     acc_ref[...] = jnp.zeros_like(acc_ref)
     ones = jnp.ones((ACC - 128, CHUNK), jnp.bfloat16)
     tile = 256
-    units = NZ + 1
+    turns = 2 * NZ
 
     def work(head, way, step_z, masked):
         lanes = pl.ds(pl.multiple_of(head * 128, 128), 128)
         below = pl.ds(pl.multiple_of(256 + head * 128, 128), 128)
-        keys = [pair_ref[step_z * NC + k, 0:256, lanes] for k in range(NC)]
-        values = [pair_ref[step_z * NC + k, below, :] for k in range(NC)]
+        keys = [pairs[step_z * NC + k, 0:256, lanes] for k in range(NC)]
+        values = [pairs[step_z * NC + k, below, :] for k in range(NC)]
         keys = jnp.concatenate(keys, axis=0)
         values = jnp.concatenate([jnp.concatenate(values, axis=1), ones], axis=0)
-        for first in range(0, COLS, tile):
+
+        def score(slot, first):
             cols = slice(first, first + tile)
             scores = jnp.dot(keys, rhs_ref[head, way, :, cols], preferred_element_type=jnp.float32)
             if masked:
@@ -417,6 +350,15 @@
                 query_x = lax.rem(x - (col // HALF) % NX + NX, NX)
                 position = (2 * query_x + c) * BLOCK + way * HALF + col % HALF
                 scores = jnp.where(position >= key, scores, -3e38)
+            score_ref[slot] = scores
+
+        score(0, 0)
+        for number in range(COLS // tile):
+            first = number * tile
+            if first + tile < COLS:
+                score((number + 1) % 2, first + tile)
+            scores = score_ref[number % 2]
+            cols = slice(first, first + tile)
             earlier = max_ref[way, 0:1, cols]
             now = jnp.maximum(earlier, jnp.max(scores, axis=0, keepdims=True))
             weights = jnp.exp2((scores - now) * EXP2_SCALE).astype(jnp.bfloat16)
@@ -430,7 +372,7 @@
         maps = pl.ds(2 * head, 2)
         device = (z, lax.rem(x + NX - k, NX), c, t)
         return remote(
-            partial.at[k, maps], parts.at[k - 1, maps],
+            partial.at[k, maps], others.at[k - 1, maps],
             p_send.at[head, k - 1], p_recv.at[head, k - 1], device,
         )
 
@@ -454,18 +396,30 @@
         for k in range(1, NX):
             x_copy(head, k).start()
 
+    def peer_copy(slot):
+        block = pairs.at[0] if slot < 7 else pairs.at[0, pl.ds(0, BLOCK), :]
+        return remote(block, block, c_send.at[slot], c_recv.at[slot], across)
+
     def unit(index, carry):
-        head = index // units
-        step = lax.rem(index, units)
-        way = jnp.where(step > z, 1, 0)
-        step_z = jnp.where(step > z, step - z - 1, step)
-        last = (step == z) | (step == units - 1)
-
-        @pl.when(last)
+        head = index // turns
+        turn = lax.rem(index, turns)
+        way = lax.rem(turn, 2)
+        near = turn // 2
+        distance = (near + 1) // 2
+        step_z = lax.rem(z + jnp.where(lax.rem(near, 2) == 1, NZ - distance, distance), NZ)
+        query_z = jnp.where(way == 0, z, NZ - 1 - z)
+        for place, slots in ((0, (0,)), (2, (1,)), (4, (2,)), (6, (3,)), (8, (4,)), (10, (5,)), (12, (6,)), (14, (7, 8))):
+
+            @pl.when(index == place)
+            def _():
+                for slot in slots:
+                    peer_copy(slot).wait_recv()
+
+        @pl.when(step_z == query_z)
         def _():
             work(head, way, step_z, True)
 
-        @pl.when(jnp.logical_not(last))
+        @pl.when(step_z < query_z)
         def _():
             work(head, way, step_z, False)
 
@@ -475,11 +429,15 @@
             def _():
                 add_relay(dz)
 
-            @pl.when(index == 2 * k + 2)
+            @pl.when(index == 2 * k + 3)
             def _():
                 finish(dz)
 
-        @pl.when(index == units - 1)
+        @pl.when(index == 7)
+        def _():
+            kv_step(4)
+
+        @pl.when(index == turns - 1)
         def _():
             send_partial(0)
             max_ref[...] = jnp.full_like(max_ref, LOW)
@@ -487,7 +445,7 @@
 
         return carry
 
-    lax.fori_loop(0, 2 * units, unit, 0)
+    lax.fori_loop(0, 2 * turns, unit, 0)
     send_partial(1)
 
     for head in range(2):
@@ -496,7 +454,7 @@
         per_map = []
         for which in range(2):
             index = 2 * head + which
-            sources = [partial.at[0, index]] + [parts.at[k, index] for k in range(NX - 1)]
+            sources = [partial.at[0, index]] + [others.at[k, index] for k in range(NX - 1)]
             totals_of, maxima = [], []
             for part in sources:
                 stats = part[128:ACC, :].astype(jnp.float32)
@@ -571,43 +529,78 @@
     ).astype(jnp.bfloat16)
 
     for k in range(2):
-        pltpu.make_async_copy(pairs[k][4].at[me], pairs[k][5].at[me], own_sem.at[k]).wait()
+        pltpu.make_async_copy(stages[k][4].at[me], stages[k][5].at[me], r_sem.at[k]).wait()
         every = pl.ds(0, NZ * group - 1)
         copy = remote(
-            pairs[k][4].at[every], pairs[k][5].at[every], out_send.at[k], out_recv.at[k], to_after
+            stages[k][4].at[every], stages[k][5].at[every], back_send.at[k], back_recv.at[k], to_after
         )
         copy.wait_recv()
         copy.wait_send()
         for dz in far:
             relay_copy(dz, k).wait_send()
             for way in range(2):
-                y_copy(dz, k, way, pairs[k][2].at[dz]).wait_send()
+                s_copy(dz, k, way, stages[k][2].at[dz]).wait_send()
     for head in range(2):
         for k in range(1, NX):
             x_copy(head, k).wait_send()
 
-
-def main_call(head_lambda, sub_gain, fmain, ftail, queries, pairs, out_weight):
+    for dz in NEAR:
+        for slot in range(3):
+            for copy in y_copies(dz, slot, own, to_after):
+                copy.wait_send()
+    for k, (source, target) in enumerate(((main_ref, xmain), (tail_ref, xtail))):
+        every = pl.ds(0, NZ * group - 1)
+        remote(
+            source.at[every], target.at[every, :, own], out_send.at[k], out_recv.at[k, 0], higher
+        ).wait_send()
+    for way in range(2):
+        for step in range(4):
+            block = pairs.at[0] if step < 3 else pairs.at[0, pl.ds(0, BLOCK), :]
+            remote(block, block, kv_send.at[way, step], kv_recv.at[way, step], higher).wait_send()
+    for slot in range(9):
+        block = pairs.at[0] if slot < 7 else pairs.at[0, pl.ds(0, BLOCK), :]
+        remote(block, block, c_send.at[slot], c_recv.at[slot], across).wait_send()
+    for slot in range(7):
+        remote(
+            parts.at[0, 0], parts.at[0, 0], q_send.at[slot], q_recv.at[slot], higher
+        ).wait_send()
+
+
+VMEM = pl.BlockSpec(memory_space=pltpu.VMEM)
+HBM = pl.BlockSpec(memory_space=pl.ANY)
+
+
+def layer_call(head_lambda, sub_gain, main, tail, pair, queries, out_weight, gate, up, down):
     dma = pltpu.SemaphoreType.DMA
-    slabs = NZ * NX * NC
-    group = NX * NC
+    slabs, group = NZ * NX * NC, NX * NC
+    units = gate.shape[1]
     rows, width = BLOCK // NT, out_weight.shape[1]
     bf16, f32 = jnp.bfloat16, jnp.float32
 
-    def both(*lead):
-        return [pltpu.VMEM((*lead, count, COLS_T), bf16) for count in (FULL, TAIL)]
+    def both(*lead, columns=COLS_T):
+        return [pltpu.VMEM((*lead, count, columns), bf16) for count in (FULL, TAIL)]
 
     return pl.pallas_call(
-        main_kernel,
+        layer_kernel,
         out_shape=(
             jax.ShapeDtypeStruct((rows, width), bf16),
             jax.ShapeDtypeStruct((slabs, FULL, COLS_T), bf16),
             jax.ShapeDtypeStruct((slabs, TAIL, COLS_T), bf16),
         ),
-        in_specs=[pl.BlockSpec(memory_space=pltpu.SMEM)] + [VMEM] * 6,
+        in_specs=[pl.BlockSpec(memory_space=pltpu.SMEM)] + [VMEM] * 6 + [HBM] * 3,
         out_specs=(VMEM,) * 3,
         scratch_shapes=[
+            *both(slabs, columns=width),
+            pltpu.VMEM((slabs * (FULL + TAIL), width), bf16),
+            pltpu.VMEM((slabs * (FULL + TAIL), units), bf16),
+            pltpu.VMEM((width, units), bf16),
+            pltpu.VMEM((width, units), bf16),
+            pltpu.VMEM((units, width), bf16),
+            *both(slabs, columns=width),
+            pltpu.VMEM((NZ * NC, 2 * BLOCK, BLOCK), bf16),
+            pltpu.VMEM((2, NX, BLOCK, HALF), bf16),
             pltpu.VMEM((2, 2, 128, COLS), bf16),
+            pltpu.VMEM((2, CHUNK, 256), f32),
             pltpu.VMEM((2, 8, COLS), f32),
             pltpu.VMEM((2, ACC, COLS), f32),
             pltpu.VMEM((NX, 4, ACC, BLOCK), bf16),
@@ -620,15 +613,17 @@
             pltpu.VMEM((2, rows // 2, width), bf16),
             pltpu.VMEM((2, rows, width), bf16),
             *both(NZ, group), *both(NZ, group), *both(2, NZ, group), *both(slabs),
+            dma((3,)), dma((4,)), dma((2,)), dma((2, NZ)), dma((3, NZ, 2)), dma((3, NZ, 2)),
+            dma((2, 4)), dma((2, 4)), dma((9,)), dma((9,)), dma((7,)), dma((7,)),
             dma((2,)), dma((2, 3)), dma((2, 3)), dma((NZ, 2)), dma((NZ, 2)),
             dma((2, NZ, 2)), dma((2, NZ, 2)), dma((2,)), dma((2,)),
             dma(()), dma(()), dma((2,)), dma((2,)), dma((2, 2)), dma((2, 2)),
         ],
         compiler_params=pltpu.CompilerParams(
-            collective_id=1, has_side_effects=True, vmem_limit_bytes=44 * 2**20
+            collective_id=0, has_side_effects=True, vmem_limit_bytes=56 * 2**20
         ),
-        name="mixer",
-    )(head_lambda, sub_gain[:, None], fmain, ftail, queries, pairs, out_weight)
+        name="layer",
+    )(head_lambda, sub_gain[:, None], main, tail, pair, queries, out_weight, gate, up, down)
 
 
 def shards(
@@ -676,11 +671,9 @@
     turned = queries.T
     halves = jnp.stack([turned[:, :HALF], turned[:, HALF:]])
 
-    fmain, ftail, pairs, parts = dispatch_call(
-        main, tail, pair, halves, gate_weight[0], up_weight[0], down_weight[0]
-    )
-    mixer_out, rmain, rtail = main_call(
-        head_lambda, sub_gain, fmain, ftail, parts, pairs, out_weight
+    mixer_out, rmain, rtail = layer_call(
+        head_lambda, sub_gain, main, tail, pair, halves, out_weight,
+        gate_weight[0], up_weight[0], down_weight[0],
     )
     returned = jnp.concatenate(
         [rmain.reshape(experts * FULL, COLS_T), rtail.reshape(experts * TAIL, COLS_T)], axis=0

time: 165 us -> 139 us (0.84); the launches traced: 163 us -> 139 us
  Pallas kernels: 145 us -> 125 us
  local copies, waits for them, and re-layouts: 12.2 us -> 6.57 us
    pallas_call x2 -> x1, Pallas kernels: 145 us -> 125 us  [layer_call(): pl.pallas_call(layer_kernel, out_shape=(jax.ShapeDtypeStruct((rows, width...]
    unnamed x30 -> x18, local copies, waits for them, and re-layouts: 10.3 us -> 1.72 us
where the time goes in v4:
time: 139 us
  Pallas kernels  125 us (90%)
  local copies, waits for them, and re-layouts  6.57 us (5%)
  other arithmetic  3.9 us (3%)
  matrix products  2.49 us (2%)
    pallas_call x1, Pallas kernels, layer_call(): pl.pallas_call(layer_kernel, out_shape=(jax.ShapeDtypeStruct((rows, width...  125 us

profile of v4, /device:TPU:2, one launch (start us, length us, event | category | flops | bytes accessed | tf_op | source)
XLA Modules:
  0.0 139.0 jit_solution(15905118519099746126)
XLA Ops:
  0.6 0.0 copy-start
  0.6 0.8 dynamic-slice
  1.5 0.8 copy.44
  2.3 0.1 eq.42
  2.4 0.9 reduce-window.6
  3.3 0.2 slice_reduce_fusion
  3.6 0.1 eq.38
  3.8 0.1 fusion.11
  3.9 0.1 reduce_sum.30
  4.0 0.1 copy.47
  4.1 0.7 compare_select_fusion
  4.8 0.1 fusion
  5.0 0.0 copy-done
  5.0 0.2 convert_element_type.23
  5.1 0.0 copy-start.2
  5.2 0.2 multiply_reduce_fusion
  5.4 0.0 copy-start.3
  5.4 0.4 convolution_convert_fusion
  5.9 0.0 copy-start.4
  5.9 0.0 copy-start.6
  5.9 0.8 slice_bitcast_fusion.main_ref
  6.7 0.7 reshape.60.tail_ref
  7.4 0.0 copy-done.2
  7.4 0.1 copy.51
  7.6 0.7 pad_maximum_fusion.1.query_ref
  8.2 0.0 copy-done.3
  8.2 0.1 copy.50
  8.3 0.0 copy-done.4
  8.3 0.7 pad_maximum_fusion.pair_ref
  9.1 0.0 copy-done.6
  9.1 0.7 copy.52.gain_ref
  9.8 0.0 copy-start.5
  9.8 125.2 %layer.1 = (bf16[64,2048]{1,0:T(8,128)(2,1)}, bf16[64,8,512]{2,1,0:T(8,128)(2,1)}, bf16[64,2,512]{2,1,0:T(2,128)(2,1)}) custom-call(f32[2]{0:T(128)} %lambda_ref.1, f32[128,1]{1,0:T(8,128)} %copy.52.gain_ref, bf16[64,8,512]{2,1,0:T(8,128)(2,1)} %slice_bitcast_fusion.main_ref, bf16[64,2,512]{2,1,0:T(2,128)(2,1)} %reshape.60.tail_ref, ...), custom_call_target="tpu_custom_call" | custom-call | tf_op jit(solution)/shard_map/layer/pallas_call | solution.py:583
  135.0 0.0 copy-start.1
  135.1 1.0 reshape.62
  136.1 0.0 copy-done.5
  136.1 0.2 select_reduce_fusion
  136.3 2.0 %convolution_convert_fusion.1 = bf16[192,512]{1,0:T(8,128)(2,1)} fusion(bf16[640,192]{0,1:T(8,128)(2,1)S(1)} %select_reduce_fusion, bf16[128,512]{1,0:T(8,128)(2,1)S(1)} %reshape.62, bf16[512,512]{1,0:T(8,128)(2,1)} %bitcast.42), kind=kOutput, calls=%fused_computation.2 | convolution fusion | flops 127139840 | bytes 1097728 | tf_op jit(solution)/shard_map/dot_general | solution.py:681
  138.3 0.0 copy-done.1
  138.3 0.7 copy.56
  (5 shorter events, 0.1 us)
Async XLA Ops:
  0.6 4.3 %copy-start = (bf16[192,2048]{1,0:T(8,128)(2,1)S(1)}, bf16[192,2048]{1,0:T(8,128)(2,1)}, u32[]{:S(2)}) copy-start(bf16[192,2048]{1,0:T(8,128)(2,1)} %param.19) | copy-start | bytes 2359300
  5.1 2.3 %copy-start.2 = (bf16[256,256]{1,0:T(8,128)(2,1)S(1)}, bf16[256,256]{1,0:T(8,128)(2,1)}, u32[]{:S(2)}) copy-start(bf16[256,256]{1,0:T(8,128)(2,1)} %param.13) | copy-start | bytes 393220
  5.4 2.8 %copy-start.3 = (bf16[256,256]{1,0:T(8,128)(2,1)S(1)}, bf16[256,256]{1,0:T(8,128)(2,1)}, u32[]{:S(2)}) copy-start(bf16[256,256]{1,0:T(8,128)(2,1)} %param.15) | copy-start | bytes 393220
  5.9 2.5 %copy-start.4 = (bf16[256,256]{1,0:T(8,128)(2,1)S(1)}, bf16[256,256]{1,0:T(8,128)(2,1)}, u32[]{:S(2)}) copy-start(bf16[256,256]{1,0:T(8,128)(2,1)} %param.14) | copy-start | bytes 393220
  5.9 3.2 %copy-start.6 = (f32[128]{0:T(128)S(1)}, f32[128]{0:T(128)}, u32[]{:S(2)}) copy-start(f32[128]{0:T(128)} %param.17) | copy-start | bytes 1540
  9.8 126.3 %copy-start.5 = (f32[192,2]{0,1:T(2,128)S(1)}, f32[192,2]{0,1:T(2,128)}, u32[]{:S(2)}) copy-start(f32[192,2]{0,1:T(2,128)} %param.22) | copy-start | bytes 4612
  135.0 3.3 %copy-start.1 = (bf16[64,2048]{1,0:T(8,128)(2,1)S(1)}, bf16[64,2048]{1,0:T(8,128)(2,1)}, u32[]{:S(2)}) copy-start(bf16[64,2048]{1,0:T(8,128)(2,1)} %get-tuple-element.12) | copy-start | bytes 786436

commit v5 on v4

--- a/solution.py
+++ b/solution.py
@@ -66,7 +66,7 @@
             device_id_type=pl.DeviceIdType.MESH,
         )
     lax.fori_loop(1, NZ * NX * NC, signal, 0)
-    pl.semaphore_wait(barrier, NZ * NX * NC + 1)
+    return barrier
 
 
 def columns_of(t):
@@ -74,9 +74,10 @@
 
 
 def layer_kernel(
-    lambda_ref, gain_ref, main_ref, tail_ref, pair_ref, query_ref, weight_ref,
-    gate_ref, up_ref, down_ref,
-    out_ref, rmain, rtail,
+    lambda_ref, gain_ref, keys_ref, values_ref, queries_ref, token_ref, norm_ref, ids_ref,
+    share_ref, weight_ref, gate_ref, up_ref, down_ref,
+    out_ref, mixed_ref,
+    main_ref, tail_ref, pair_ref, query_ref, combine_ref, rmain, rtail,
     xmain, xtail, taken, hidden, gate, up, down, fmain, ftail, pairs, parts,
     rhs_ref, score_ref, max_ref, acc_ref, partial, others,
     attended, upper_send, upper_recv, blocks, relayed, totals, arrived_y,
@@ -91,19 +92,65 @@
     group = NX * NC
     after, before = lax.rem(t + 1, NT), lax.rem(t + NT - 1, NT)
     own = columns_of(t)
+    weight_copies = [
+        pltpu.make_async_copy(source, target, w_sem.at[k])
+        for k, (source, target) in enumerate(((gate_ref, gate), (up_ref, up), (down_ref, down)))
+    ]
+    for copy in weight_copies:
+        copy.start()
+    barrier = greet_all(z, x, c, t)
+
+    wide = token_ref[...].astype(jnp.float32)
+    scale = lax.rsqrt(jnp.mean(wide * wide, axis=-1, keepdims=True) + EPS)
+    normed_own = token_ref[:, own].astype(jnp.float32) * scale * norm_ref[:, own]
+    normed_own = normed_own.astype(jnp.bfloat16)
+    tokens, experts = token_ref.shape[0], NZ * group
+    spots = experts * (FULL + TAIL)
+    earlier_token = lax.broadcasted_iota(jnp.int32, (tokens, tokens), 1) < (
+        lax.broadcasted_iota(jnp.int32, (tokens, tokens), 0)
+    )
+    earlier_token = jnp.where(earlier_token, 1.0, 0.0).astype(jnp.bfloat16)
+    expert = lax.broadcasted_iota(jnp.int32, (tokens, experts), 1)
+    spot = lax.broadcasted_iota(jnp.int32, (tokens, spots), 1)
+    counted = jnp.zeros((1, experts), jnp.float32)
+    chosen, combine = jnp.zeros((tokens, spots), jnp.float32), 0.0
+    for route in range(2):
+        named = ids_ref[:, route : route + 1]
+        onehot = jnp.where(expert == named, 1.0, 0.0)
+        rank = counted + jnp.dot(
+            earlier_token, onehot.astype(jnp.bfloat16), preferred_element_type=jnp.float32
+        )
+        slot = jnp.sum(rank * onehot, axis=1, keepdims=True)
+        counted = counted + jnp.sum(onehot, axis=0, keepdims=True)
+        number = named.astype(jnp.float32)
+        place = jnp.where(
+            slot < FULL, number * FULL + slot, experts * FULL + number * TAIL + slot - FULL
+        )
+        hit = spot.astype(jnp.float32) == place
+        chosen = jnp.where(hit, 1.0, chosen)
+        combine = combine + jnp.where(hit, share_ref[:, route : route + 1], 0.0)
+    combine_ref[...] = combine.astype(jnp.bfloat16)
+    outgoing = lax.dot_general(
+        chosen.astype(jnp.bfloat16), normed_own,
+        (((0,), (0,)), ((), ())), preferred_element_type=jnp.float32,
+    ).astype(jnp.bfloat16)
+    main_ref[...] = outgoing[: experts * FULL].reshape(experts, FULL, COLS_T)
+    tail_ref[...] = outgoing[experts * FULL :].reshape(experts, TAIL, COLS_T)
+    pair_ref[0:BLOCK, :] = keys_ref[...]
+    pair_ref[BLOCK:, :] = values_ref[...].T
+    turned = queries_ref[...].T
+    query_ref[0] = turned[:, :HALF]
+    query_ref[1] = turned[:, HALF:]
+    pl.semaphore_wait(barrier, NZ * NX * NC + 1)
+
     own_copies = [
         pltpu.make_async_copy(main_ref.at[me], xmain.at[me, :, own], own_sem.at[0]),
         pltpu.make_async_copy(tail_ref.at[me], xtail.at[me, :, own], own_sem.at[1]),
         pltpu.make_async_copy(pair_ref, pairs.at[z * NC + c], own_sem.at[2]),
         pltpu.make_async_copy(query_ref.at[0], parts.at[0, 0], own_sem.at[3]),
     ]
-    weight_copies = [
-        pltpu.make_async_copy(source, target, w_sem.at[k])
-        for k, (source, target) in enumerate(((gate_ref, gate), (up_ref, up), (down_ref, down)))
-    ]
-    for copy in own_copies + weight_copies:
+    for copy in own_copies:
         copy.start()
-    greet_all(z, x, c, t)
 
     for dz in (1, 7, 2, 6, 3, 5, 4, 0):
         to_z = lax.rem(z + dz, NZ)
@@ -448,6 +495,7 @@
     lax.fori_loop(0, 2 * turns, unit, 0)
     send_partial(1)
 
+    gain_col = jnp.broadcast_to(gain_ref[...], (128, 128)).T[:, 0:1]
     for head in range(2):
         for k in range(1, NX):
             x_copy(head, k).wait_recv()
@@ -469,7 +517,7 @@
             per_map.append(numerator / total)
         contrast = per_map[0] - lambda_ref[head] * per_map[1]
         square = jnp.mean(contrast * contrast, axis=0, keepdims=True)
-        normed = contrast * lax.rsqrt(square + EPS) * gain_ref[...]
+        normed = contrast * lax.rsqrt(square + EPS) * gain_col
         normed = normed.astype(jnp.bfloat16)
         attended[head * 128 : (head + 1) * 128, :] = normed[:, :HALF]
         upper_send[head * 128 : (head + 1) * 128, :] = normed[:, HALF:]
@@ -516,6 +564,29 @@
             mine.astype(jnp.float32) + relayed[way].astype(jnp.float32)
         ).astype(jnp.bfloat16)
         mix_copy(way, way, totals.at[way]).start()
+    for k in range(2):
+        pltpu.make_async_copy(stages[k][4].at[me], stages[k][5].at[me], r_sem.at[k]).wait()
+        every = pl.ds(0, NZ * group - 1)
+        copy = remote(
+            stages[k][4].at[every], stages[k][5].at[every], back_send.at[k], back_recv.at[k], to_after
+        )
+        copy.wait_recv()
+        copy.wait_send()
+        for dz in far:
+            relay_copy(dz, k).wait_send()
+            for way in range(2):
+                s_copy(dz, k, way, stages[k][2].at[dz]).wait_send()
+    full = experts * FULL
+    mixed_ref[...] = (
+        jnp.dot(
+            combine_ref[:, :full], rmain[...].reshape(full, COLS_T),
+            preferred_element_type=jnp.float32,
+        )
+        + jnp.dot(
+            combine_ref[:, full:], rtail[...].reshape(spots - full, COLS_T),
+            preferred_element_type=jnp.float32,
+        )
+    ).astype(jnp.bfloat16)
     for way in range(2):
         for part in range(2):
             copy = mix_copy(way, part, totals.at[way])
@@ -528,18 +599,6 @@
         + arrived_y[1].astype(jnp.float32)
     ).astype(jnp.bfloat16)
 
-    for k in range(2):
-        pltpu.make_async_copy(stages[k][4].at[me], stages[k][5].at[me], r_sem.at[k]).wait()
-        every = pl.ds(0, NZ * group - 1)
-        copy = remote(
-            stages[k][4].at[every], stages[k][5].at[every], back_send.at[k], back_recv.at[k], to_after
-        )
-        copy.wait_recv()
-        copy.wait_send()
-        for dz in far:
-            relay_copy(dz, k).wait_send()
-            for way in range(2):
-                s_copy(dz, k, way, stages[k][2].at[dz]).wait_send()
     for head in range(2):
         for k in range(1, NX):
             x_copy(head, k).wait_send()
@@ -570,11 +629,15 @@
 HBM = pl.BlockSpec(memory_space=pl.ANY)
 
 
-def layer_call(head_lambda, sub_gain, main, tail, pair, queries, out_weight, gate, up, down):
+def layer_call(
+    queries, key_rows, value_rows, head_lambda, sub_gain, out_weight, expert_input, norm_gain,
+    route_ids, route_weight, gate, up, down,
+):
     dma = pltpu.SemaphoreType.DMA
     slabs, group = NZ * NX * NC, NX * NC
     units = gate.shape[1]
     rows, width = BLOCK // NT, out_weight.shape[1]
+    tokens = expert_input.shape[0]
     bf16, f32 = jnp.bfloat16, jnp.float32
 
     def both(*lead, columns=COLS_T):
@@ -584,12 +647,16 @@
         layer_kernel,
         out_shape=(
             jax.ShapeDtypeStruct((rows, width), bf16),
-            jax.ShapeDtypeStruct((slabs, FULL, COLS_T), bf16),
-            jax.ShapeDtypeStruct((slabs, TAIL, COLS_T), bf16),
+            jax.ShapeDtypeStruct((tokens, COLS_T), bf16),
         ),
-        in_specs=[pl.BlockSpec(memory_space=pltpu.SMEM)] + [VMEM] * 6 + [HBM] * 3,
-        out_specs=(VMEM,) * 3,
+        in_specs=[pl.BlockSpec(memory_space=pltpu.SMEM)] + [VMEM] * 9 + [HBM] * 3,
+        out_specs=(VMEM,) * 2,
         scratch_shapes=[
+            *both(slabs),
+            pltpu.VMEM((2 * BLOCK, BLOCK), bf16),
+            pltpu.VMEM((2, BLOCK, HALF), bf16),
+            pltpu.VMEM((tokens, slabs * (FULL + TAIL)), bf16),
+            *both(slabs),
             *both(slabs, columns=width),
             pltpu.VMEM((slabs * (FULL + TAIL), width), bf16),
             pltpu.VMEM((slabs * (FULL + TAIL), units), bf16),
@@ -623,7 +690,10 @@
             collective_id=0, has_side_effects=True, vmem_limit_bytes=56 * 2**20
         ),
         name="layer",
-    )(head_lambda, sub_gain[:, None], main, tail, pair, queries, out_weight, gate, up, down)
+    )(
+        head_lambda, sub_gain[None, :], key_rows, value_rows, queries, expert_input,
+        norm_gain[None, :], route_ids, route_weight, out_weight, gate, up, down,
+    )
 
 
 def shards(
@@ -641,50 +711,10 @@
     up_weight,
     down_weight,
 ):
-    rows_here, model_width = expert_input.shape
-    experts = NZ * NX * NC
-    top_count = route_ids.shape[1]
-    slots = experts * (FULL + TAIL)
-    wide_rows = expert_input.astype(jnp.float32)
-    normed = (
-        wide_rows
-        * lax.rsqrt(jnp.mean(wide_rows * wide_rows, axis=-1, keepdims=True) + EPS)
-        * norm_gain
-    ).astype(jnp.bfloat16)
-    flat_ids = route_ids.reshape(-1)
-    onehot = (flat_ids[:, None] == jnp.arange(experts, dtype=jnp.int32)[None, :]).astype(jnp.int32)
-    rank_before = jnp.cumsum(onehot, axis=0) - onehot
-    slot = jnp.sum(rank_before * onehot, axis=1)
-    buffer_pos = jnp.where(
-        slot < FULL,
-        flat_ids * FULL + slot,
-        experts * FULL + flat_ids * TAIL + slot - FULL,
-    ).reshape(rows_here, top_count)
-    matches = buffer_pos[None, :, :] == jnp.arange(slots, dtype=jnp.int32)[:, None, None]
-    dispatch = jnp.any(matches, axis=-1).astype(jnp.bfloat16)
-    combine = jnp.sum(jnp.where(matches, route_weight[None, :, :], 0.0), axis=-1)
-    own_cols = lax.dynamic_slice_in_dim(normed, lax.axis_index("tp") * COLS_T, COLS_T, 1)
-    outgoing = jnp.dot(dispatch, own_cols, preferred_element_type=jnp.float32).astype(jnp.bfloat16)
-    main = outgoing[: experts * FULL].reshape(experts, FULL, COLS_T)
-    tail = outgoing[experts * FULL :].reshape(experts, TAIL, COLS_T)
-    pair = jnp.concatenate([key_rows, value_rows.T], axis=0)
-    turned = queries.T
-    halves = jnp.stack([turned[:, :HALF], turned[:, HALF:]])
-
-    mixer_out, rmain, rtail = layer_call(
-        head_lambda, sub_gain, main, tail, pair, halves, out_weight,
-        gate_weight[0], up_weight[0], down_weight[0],
+    return layer_call(
+        queries, key_rows, value_rows, head_lambda, sub_gain, out_weight, expert_input, norm_gain,
+        route_ids, route_weight, gate_weight[0], up_weight[0], down_weight[0],
     )
-    returned = jnp.concatenate(
-        [rmain.reshape(experts * FULL, COLS_T), rtail.reshape(experts * TAIL, COLS_T)], axis=0
-    )
-    mixed = lax.dot_general(
-        combine,
-        returned.astype(jnp.float32),
-        (((0,), (0,)), ((), ())),
-        preferred_element_type=jnp.float32,
-    )
-    return (mixer_out, mixed.astype(jnp.bfloat16))
 
 
 def solution(mesh):

time: 139 us -> 132 us (0.950)
  other arithmetic: 3.9 us -> 0 us
  matrix products: 2.49 us -> 0 us
    unnamed x18 -> x4, local copies, waits for them, and re-layouts: 1.72 us -> 6.17 us
    reshape x3 -> x0, local copies, waits for them, and re-layouts: 2.54 us -> none  [the longest x1 1 us: shards(): rtail.reshape(experts * TAIL, COLS_T)]
    dot_general x2 -> x0, matrix products: 2.49 us -> none  [the longest x1 2.04 us: shards(): lax.dot_general(combine, returned.astype(jnp.float32), (((0,), (0,)), (()...]
    another operation x3 -> x0, other arithmetic: 1.61 us -> none
where the time goes in v5:
time: 132 us
  Pallas kernels  125 us (95%)
  local copies, waits for them, and re-layouts  6.17 us (5%)
    pallas_call x1, Pallas kernels, layer_call(): pl.pallas_call(layer_kernel, out_shape=(jax.ShapeDtypeStruct((rows, width...  125 us
    unnamed x4, local copies, waits for them, and re-layouts  6.17 us

profile of v5, /device:TPU:2, one launch (start us, length us, event | category | flops | bytes accessed | tf_op | source)
XLA Modules:
  0.0 131.9 jit_solution(6534350765268157579)
XLA Ops:
  0.6 1.4 %copy.15.ids_ref = s32[192,2]{1,0:T(8,128)} copy(s32[192,2]{0,1:T(2,128)} %param.21) | data formatting | bytes 3072 | tf_op args[8]
  2.1 1.4 %copy.16.share_ref = f32[192,2]{1,0:T(8,128)} copy(f32[192,2]{0,1:T(2,128)} %param.22) | data formatting | bytes 3072 | tf_op args[9]
  3.5 125.1 %layer.1 = (bf16[64,2048]{1,0:T(8,128)(2,1)}, bf16[192,512]{1,0:T(8,128)(2,1)}) custom-call(f32[2]{0:T(128)} %lambda_ref.1, f32[1,128]{1,0:T(1,128)} %bitcast.9, bf16[256,256]{1,0:T(8,128)(2,1)} %keys_ref.1, bf16[256,256]{1,0:T(8,128)(2,1)} %values_ref.1, bf16[256,256]{1,0:T(8,128)(2,1)} %queries_ref.1, bf16[192,2048]{1,0:T(8,128)(2,1)} %token_ref.1, ...), custom_call_target="tpu_custom_call" | custom-call | tf_op jit(solution)/shard_map/layer/pallas_call | solution.py:646
  128.6 1.7 %copy.19 = bf16[64,2048]{1,0:T(8,128)(2,1)} copy(bf16[64,2048]{1,0:T(8,128)(2,1)} %get-tuple-element.4) | data formatting | bytes 524288
  130.3 1.6 %copy.20 = bf16[192,512]{1,0:T(8,128)(2,1)} copy(bf16[192,512]{1,0:T(8,128)(2,1)} %get-tuple-element.5) | data formatting | bytes 393216

commit v6 on v5

--- a/solution.py
+++ b/solution.py
@@ -114,8 +114,9 @@
     spot = lax.broadcasted_iota(jnp.int32, (tokens, spots), 1)
     counted = jnp.zeros((1, experts), jnp.float32)
     chosen, combine = jnp.zeros((tokens, spots), jnp.float32), 0.0
+    names, shares = ids_ref[...].T, share_ref[...].T
     for route in range(2):
-        named = ids_ref[:, route : route + 1]
+        named = names[:, route : route + 1]
         onehot = jnp.where(expert == named, 1.0, 0.0)
         rank = counted + jnp.dot(
             earlier_token, onehot.astype(jnp.bfloat16), preferred_element_type=jnp.float32
@@ -128,7 +129,7 @@
         )
         hit = spot.astype(jnp.float32) == place
         chosen = jnp.where(hit, 1.0, chosen)
-        combine = combine + jnp.where(hit, share_ref[:, route : route + 1], 0.0)
+        combine = combine + jnp.where(hit, shares[:, route : route + 1], 0.0)
     combine_ref[...] = combine.astype(jnp.bfloat16)
     outgoing = lax.dot_general(
         chosen.astype(jnp.bfloat16), normed_own,
@@ -692,7 +693,7 @@
         name="layer",
     )(
         head_lambda, sub_gain[None, :], key_rows, value_rows, queries, expert_input,
-        norm_gain[None, :], route_ids, route_weight, out_weight, gate, up, down,
+        norm_gain[None, :], route_ids.T, route_weight.T, out_weight, gate, up, down,
     )
 
 

time: 132 us -> 129 us (0.977)
  local copies, waits for them, and re-layouts: 6.17 us -> 3.29 us
    unnamed x4 -> x2, local copies, waits for them, and re-layouts: 6.17 us -> 3.29 us
where the time goes in v6:
time: 129 us
  Pallas kernels  125 us (97%)
  local copies, waits for them, and re-layouts  3.29 us (3%)
    pallas_call x1, Pallas kernels, layer_call(): pl.pallas_call(layer_kernel, out_shape=(jax.ShapeDtypeStruct((rows, width...  125 us
    unnamed x2, local copies, waits for them, and re-layouts  3.29 us

profile of v6, /device:TPU:2, one launch (start us, length us, event | category | flops | bytes accessed | tf_op | source)
XLA Modules:
  0.0 129.1 jit_solution(5295373187055445032)
XLA Ops:
  0.6 125.2 %layer.1 = (bf16[64,2048]{1,0:T(8,128)(2,1)}, bf16[192,512]{1,0:T(8,128)(2,1)}) custom-call(f32[2]{0:T(128)} %lambda_ref.1, f32[1,128]{1,0:T(1,128)} %bitcast.13, bf16[256,256]{1,0:T(8,128)(2,1)} %keys_ref.1, bf16[256,256]{1,0:T(8,128)(2,1)} %values_ref.1, bf16[256,256]{1,0:T(8,128)(2,1)} %queries_ref.1, bf16[192,2048]{1,0:T(8,128)(2,1)} %token_ref.1, ...), custom_call_target="tpu_custom_call" | custom-call | tf_op jit(solution)/shard_map/layer/pallas_call | solution.py:647
  125.8 1.7 %copy.17 = bf16[64,2048]{1,0:T(8,128)(2,1)} copy(bf16[64,2048]{1,0:T(8,128)(2,1)} %get-tuple-element.4) | data formatting | bytes 524288
  127.5 1.6 %copy.18 = bf16[192,512]{1,0:T(8,128)(2,1)} copy(bf16[192,512]{1,0:T(8,128)(2,1)} %get-tuple-element.5) | data formatting | bytes 393216
